TPU v7x, 32 devices: a whole 2x2x4 slice. The times are simulated.
32 devices in a mesh: sp: 8 (over z, x), tp: 4 (over y, core).
Axes of the slice: x: 2, y: 2, z: 4, core: 2. Of those that a mesh axis runs over, the one named last changes fastest.
Arguments:
- cot_out: bfloat16 [2048, 2048], P('sp', 'tp'), may hold values from -6 to 6
- route_ids: int32 [2048, 2], P('sp'), may hold values from 0 to 7, all different within a row; in each aligned block of 256 rows (0 to 255, 256 to 511, ...) at most 96 rows name the same one
- route_weight: float32 [2048, 2], P('sp'), may hold values from 0.1 to 1
- expert_inputs: bfloat16 [8, 768, 2048], P('sp'), may hold values from -48 to 48
- w_gate: bfloat16 [8, 2048, 1024], P('sp', None, 'tp'), may hold values from -0.125 to 0.125
- w_up: bfloat16 [8, 2048, 1024], P('sp', None, 'tp'), may hold values from -0.125 to 0.125
- w_down: bfloat16 [8, 1024, 2048], P('sp', 'tp'), may hold values from -0.1875 to 0.1875
- w_proj: bfloat16 [2048, 2048], P('tp'), may hold values from -0.125 to 0.125
- conv_out: bfloat16 [2048, 2048], P('sp', 'tp'), may hold values from -6 to 6
- channel_norm_gain: float32 [2048], P('tp'), may hold values from 0.1 to 1.9
- taps: float32 [31, 2048], P(None, 'tp'), may hold values from -1 to 1
- value_pre: bfloat16 [2048, 2048], P('sp', 'tp'), may hold values from -6 to 6
- gate_pre: bfloat16 [2048, 2048], P('sp', 'tp'), may hold values from -6 to 6
Outputs:
- grad_gate_w: bfloat16 [8, 2048, 1024], P('sp', None, 'tp')
- grad_up_w: bfloat16 [8, 2048, 1024], P('sp', None, 'tp')
- grad_down_w: bfloat16 [8, 1024, 2048], P('sp', 'tp')
- grad_proj: float32 [2048, 2048], P(('tp', 'sp'))
- grad_value: bfloat16 [2048, 2048], P('sp', 'tp')
- grad_gate: bfloat16 [2048, 2048], P('sp', 'tp')
Inputs may be any that keep to these rules, and one draw needn't show every extreme that they name: `route_ids`: among the tokens of one index of sp no expert is chosen more than 96 times, a bound that some block reaches; a token's experts differ.
All inputs are finite; a program needn't handle non-finite values.
Results may differ from a plain program's by a relative error of at most 0.012.
Values may be sent and summed in bfloat16 or wider, within the bound.
A program may use at most 128 MiB of HBM per device.

v0:
```python
import jax
import jax.numpy as jnp
from jax import lax
from jax.sharding import PartitionSpec as P

clamp_limit = 7.0
swish_alpha = 1.702
norm_epsilon = 1e-05


def passed_along(value, axis, steps):
    count = lax.axis_size(axis)
    leading, last = (max(0, -steps), min(count, count - steps))
    return lax.ppermute(value, axis, [(source, source + steps) for source in range(leading, last)])


def per_device(
    cot_out,
    route_ids,
    route_weight,
    expert_inputs,
    w_gate,
    w_up,
    w_down,
    w_proj,
    conv_out,
    channel_norm_gain,
    taps,
    value_pre,
    gate_pre,
):
    group_size = lax.axis_size("sp")
    narrow_size = lax.axis_size("tp")
    tok_rows = cot_out.shape[0]
    chosen = route_ids.shape[1]
    slot_rows = expert_inputs.shape[1]
    capacity = slot_rows // group_size
    model_width = expert_inputs.shape[2]
    local_cols = cot_out.shape[1]
    flat_ids = route_ids.reshape(-1)
    expert_hot = (flat_ids[:, None] == jnp.arange(group_size, dtype=jnp.int32)[None, :]).astype(
        jnp.int32
    )
    earlier = jnp.sum((jnp.cumsum(expert_hot, axis=0) - expert_hot) * expert_hot, axis=1)
    dest_rows = flat_ids * capacity + earlier
    flat_weight = route_weight.reshape(-1)[:, None]
    scaled = (flat_weight * jnp.repeat(cot_out, chosen, axis=0).astype(jnp.float32)).astype(
        jnp.bfloat16
    )
    outgoing = (
        jnp.zeros((group_size * capacity, local_cols), jnp.bfloat16).at[dest_rows].set(scaled)
    )
    moved = lax.all_to_all(
        outgoing.reshape(group_size, capacity, local_cols),
        "sp",
        split_axis=0,
        concat_axis=0,
        tiled=True,
    )
    arrived = lax.all_gather(moved, "tp", axis=2, tiled=True)
    rows_cot = arrived.reshape(slot_rows, model_width)
    rows_in = expert_inputs[0]
    gate_weight = w_gate[0]
    up_weight = w_up[0]
    down_weight = w_down[0]
    gate_lin = jnp.dot(rows_in, gate_weight, preferred_element_type=jnp.float32)
    up_lin = jnp.dot(rows_in, up_weight, preferred_element_type=jnp.float32)
    gate_c = jnp.minimum(gate_lin, clamp_limit)
    up_c = jnp.clip(up_lin, -clamp_limit, clamp_limit)
    sigma = jax.nn.sigmoid(swish_alpha * gate_c)
    act = ((up_c + 1.0) * gate_c * sigma).astype(jnp.bfloat16)
    grad_down = jnp.dot(act.T, rows_cot, preferred_element_type=jnp.float32).astype(jnp.bfloat16)
    d_act = jnp.dot(rows_cot, down_weight.T, preferred_element_type=jnp.float32)
    up_open = ((up_lin > -clamp_limit) & (up_lin < clamp_limit)).astype(jnp.float32)
    gate_open = (gate_lin < clamp_limit).astype(jnp.float32)
    d_up = (d_act * gate_c * sigma * up_open).astype(jnp.bfloat16)
    d_gate = (
        d_act * (up_c + 1.0) * (sigma + swish_alpha * gate_c * sigma * (1.0 - sigma)) * gate_open
    ).astype(jnp.bfloat16)
    grad_gate_part = jnp.dot(rows_in.T, d_gate, preferred_element_type=jnp.float32).astype(
        jnp.bfloat16
    )
    grad_up_part = jnp.dot(rows_in.T, d_up, preferred_element_type=jnp.float32).astype(jnp.bfloat16)
    partial_value = jnp.dot(d_gate, gate_weight.T, preferred_element_type=jnp.float32)
    partial_value = partial_value + jnp.dot(d_up, up_weight.T, preferred_element_type=jnp.float32)
    input_grad = lax.psum_scatter(
        partial_value.astype(jnp.bfloat16), "tp", scatter_dimension=1, tiled=True
    )
    coming = lax.all_to_all(
        input_grad.reshape(group_size, capacity, local_cols),
        "sp",
        split_axis=0,
        concat_axis=0,
        tiled=True,
    )
    picked = coming.reshape(group_size * capacity, local_cols)[dest_rows].astype(jnp.float32)
    summed = jnp.sum(picked.reshape(tok_rows, chosen, local_cols), axis=1)
    mix_grad = (cot_out.astype(jnp.float32) + summed).astype(jnp.bfloat16)
    mix_full = lax.all_gather(mix_grad, "tp", axis=1, tiled=True)
    convolution_filter = conv_out.astype(jnp.float32)
    channel_total = local_cols * narrow_size
    first_sum, square_sum = lax.psum(
        (
            jnp.sum(convolution_filter, axis=1),
            jnp.sum(convolution_filter * convolution_filter, axis=1),
        ),
        "tp",
    )
    channel_mean = (first_sum / channel_total)[:, None]
    var = (square_sum / channel_total)[:, None] - channel_mean * channel_mean
    inverse_deviation = lax.rsqrt(var + norm_epsilon)
    normalized_input = (convolution_filter - channel_mean) * inverse_deviation
    normalized_output = normalized_input * channel_norm_gain[None, :]
    sigma_conv = jax.nn.sigmoid(normalized_output)
    act_conv = (normalized_output * sigma_conv).astype(jnp.bfloat16)
    grad_proj = lax.psum_scatter(
        lax.dot_general(
            act_conv, mix_full, (((0,), (0,)), ((), ())), preferred_element_type=jnp.float32
        ),
        "sp",
        scatter_dimension=0,
        tiled=True,
    )
    d_act_conv = jnp.dot(mix_full, w_proj.T, preferred_element_type=jnp.float32)
    normalized_gradient = (
        d_act_conv
        * sigma_conv
        * (1.0 + normalized_output * (1.0 - sigma_conv))
        * channel_norm_gain[None, :]
    )
    first_term_gradient, second_term_gradient = lax.psum(
        (
            jnp.sum(normalized_gradient, axis=1),
            jnp.sum(normalized_gradient * normalized_input, axis=1),
        ),
        "tp",
    )
    convolution_gradient = inverse_deviation * (
        normalized_gradient
        - (first_term_gradient / channel_total)[:, None]
        - normalized_input * (second_term_gradient / channel_total)[:, None]
    )
    reach = taps.shape[0]
    following = passed_along(convolution_gradient[: reach - 1], "sp", -1)
    extended = jnp.concatenate([convolution_gradient, following], axis=0)
    d_glu = jnp.zeros_like(convolution_gradient)
    for offset in range(reach):
        begin = reach - 1 - offset
        d_glu = d_glu + taps[offset][None, :] * extended[begin : begin + tok_rows]
    gate_sig = jax.nn.sigmoid(gate_pre.astype(jnp.float32))
    grad_value = (d_glu * gate_sig).astype(jnp.bfloat16)
    grad_gate = (d_glu * value_pre.astype(jnp.float32) * gate_sig * (1.0 - gate_sig)).astype(
        jnp.bfloat16
    )
    return (
        grad_gate_part[None],
        grad_up_part[None],
        grad_down[None],
        grad_proj,
        grad_value,
        grad_gate,
    )


def solution(mesh):
    return jax.shard_map(
        per_device,
        mesh=mesh,
        in_specs=(
            P("sp", "tp"),
            P("sp", None),
            P("sp", None),
            P("sp", None, None),
            P("sp", None, "tp"),
            P("sp", None, "tp"),
            P("sp", "tp", None),
            P("tp", None),
            P("sp", "tp"),
            P("tp"),
            P(None, "tp"),
            P("sp", "tp"),
            P("sp", "tp"),
        ),
        out_specs=(
            P("sp", None, "tp"),
            P("sp", None, "tp"),
            P("sp", "tp", None),
            P(("tp", "sp"), None),
            P("sp", "tp"),
            P("sp", "tp"),
        ),
        check_vma=False,
    )
```

profile of v0, /device:TPU:0, one launch (start us, length us, event | category | flops | bytes accessed | tf_op | source)
XLA Modules:
  0.0 273.6 jit_solution(459320773826798020)
XLA Ops:
  11.0 2.2 broadcast_in_dim.11
  13.2 2.9 %convert_element_type.78 = f32[512,512]{1,0:T(8,128)} reshape(f32[256,2,512]{2,1,0:T(2,128)} %broadcast_in_dim.11) | data formatting | bytes 2097152 | tf_op jit(solution)/shard_map/convert_element_type | solution.py:47
  16.5 4.1 %scatter_custom_fusion = bf16[768,512]{1,0:T(8,128)(2,1)} fusion(s32[512]{0:T(512)S(1)} %bitcast.129, f32[512,512]{1,0:T(8,128)} %convert_element_type.78, f32[512]{0:T(512)S(1)} %mul.447, bf16[]{:T(256)} %constant.12.clone.1), kind=kCustom, calls=%fused_computation.198 | custom fusion | flops 524288 | bytes 1837058 | tf_op jit(solution)/shard_map/scatter | solution.py:51
  20.5 27.5 %all_to_all.10 = bf16[8,96,512]{2,1,0:T(8,128)(2,1)} all-to-all(bf16[8,96,512]{2,1,0:T(8,128)(2,1)} %bitcast.96), channel_id=1, replica_groups=mesh['sp'=8,'tp'=4] {'sp'}, dimensions={0} | all-to-all | bytes 1572864 | tf_op jit(solution)/shard_map/all_to_all | solution.py:53
  48.1 3.2 %fusion.4 = f32[768,256]{1,0:T(8,128)} fusion(bf16[1,768,2048]{2,1,0:T(8,128)(2,1)S(1)} %copy-done, bf16[1,2048,256]{2,1,0:T(8,128)(2,1)} %param.18), kind=kOutput, calls=%fused_computation.36 | convolution fusion | flops 805306368 | bytes 4980736 | tf_op jit(solution)/shard_map/dot_general | solution.py:67
  53.2 22.5 %all-gather.3.cloned.1.call-done = bf16[8,96,2048]{2,1,0:T(8,128)(2,1)} async-done(((bf16[8,96,512]{2,1,0:T(8,128)(2,1)}), bf16[8,96,2048]{2,1,0:T(8,128)(2,1)}) %all-gather.3.cloned.1.call-update) | async-done | bytes 3145744 | tf_op jit(solution)/shard_map/all_gather | solution.py:60
  75.8 4.1 %select_convert_fusion = (bf16[768,256]{1,0:T(8,128)(2,1)S(1)}, bf16[768,256]{1,0:T(8,128)(2,1)S(1)}) fusion(f32[768,256]{1,0:T(8,128)} %fusion.4, f32[768,256]{1,0:T(8,128)} %fusion.6, bf16[768,2048]{1,0:T(8,128)(2,1)} %bitcast.132, bf16[1,256,2048]{2,1,0:T(8,128)(2,1)} %param.19), kind=kOutput, calls=%fused_computation.61 | convolution fusion | flops 809828352 | bytes 6553600 | tf_op jit(solution)/shard_map/dot_general | solution.py:73
  81.4 2.7 add_convert_fusion
  84.1 37.9 %reduce-scatter.3.cloned.1.call-done = bf16[768,512]{1,0:T(8,128)(2,1)} async-done(((bf16[768,2048]{1,0:T(8,128)(2,1)}), bf16[768,512]{1,0:T(8,128)(2,1)}) %reduce-scatter.3.cloned.1.call-update) | async-done | bytes 786448 | tf_op jit(solution)/shard_map/reduce_scatter | solution.py:86
  122.0 5.5 %all-to-all-start.1 = ((bf16[8,96,512]{2,1,0:T(8,128)(2,1)}), bf16[8,96,512]{2,1,0:T(8,128)(2,1)}, u32[]{:S(2)}, u32[]{:S(2)}) async-start(bf16[8,96,512]{2,1,0:T(8,128)(2,1)} %bitcast.97), calls=%async_computation.2 | async-start | bytes 1572864 | tf_op jit(solution)/shard_map/all_to_all | solution.py:89
  127.8 19.9 %all-to-all-done.1 = bf16[8,96,512]{2,1,0:T(8,128)(2,1)} async-done(((bf16[8,96,512]{2,1,0:T(8,128)(2,1)}), bf16[8,96,512]{2,1,0:T(8,128)(2,1)}, u32[]{:S(2)}, u32[]{:S(2)}) %all-to-all-start.1) | async-done | bytes 786464 | tf_op jit(solution)/shard_map/all_to_all | solution.py:89
  147.7 3.9 %gather_fusion = bf16[512,512]{1,0:T(8,128)(2,1)} fusion(bf16[768,512]{1,0:T(8,128)(2,1)} %bitcast.16, s32[1024]{0:T(1024)S(1)} %pad_clamp_fusion), kind=kCustom, calls=%fused_computation | custom fusion | bytes 1050624 | tf_op jit(solution)/shard_map/gather | solution.py:96
  151.6 2.7 reshape.91
  154.3 3.3 %reduce_sum.60 = f32[256,512]{1,0:T(8,128)} reduce(f32[256,2,512]{2,1,0:T(2,128)} %reshape.91, f32[]{:T(128)} %constant.33.clone.1), dimensions={1}, to_apply=%region_9.10 | reduce | flops 131072 | bytes 1572868 | tf_op jit(solution)/shard_map/reduce_sum | solution.py:97
  159.7 5.9 %all-reduce.1 = (f32[256]{0:T(256)S(1)}, f32[256]{0:T(256)S(1)}) all-reduce(f32[256]{0:T(256)S(1)} %get-tuple-element.21, f32[256]{0:T(256)S(1)} %get-tuple-element.20), channel_id=1, replica_groups=mesh['sp'=8,'tp'=4] {'tp'}, use_global_device_ids=true, to_apply=%region_7.8 | all-reduce | flops 512 | bytes 4096 | tf_op jit(solution)/shard_map/psum | solution.py:102
  165.6 8.7 %all-gather.5.cloned.1.call-done = bf16[256,2048]{1,0:T(8,128)(2,1)} async-done(((bf16[256,512]{1,0:T(8,128)(2,1)}), bf16[256,2048]{1,0:T(8,128)(2,1)}) %all-gather.5.cloned.1.call-update) | async-done | bytes 1048592 | tf_op jit(solution)/shard_map/all_gather | solution.py:99
  174.3 4.1 %fusion.142 = f32[512,2048]{1,0:T(8,128)} fusion(bf16[256,2048]{1,0:T(8,128)(2,1)} %all-gather.5.cloned.1.call-done, bf16[256,512]{1,0:T(8,128)(2,1)S(1)} %copy-done.1, f32[512]{0:T(512)S(1)} %copy-done.11, f32[256]{0:T(256)S(1)} %get-tuple-element.62, f32[256]{0:T(256)S(1)} %get-tuple-element.61), kind=kOutput, calls=%fused_computation.211 | convolution fusion | flops 538050560 | bytes 5509120 | tf_op jit(solution)/shard_map/dot_general | solution.py:117
  180.5 3.1 %fusion.18 = bf16[1,2048,256]{1,2,0:T(8,128)(2,1)} fusion(bf16[768,256]{1,0:T(8,128)(2,1)} %copy-done.3, bf16[1,768,2048]{2,1,0:T(8,128)(2,1)S(1)} %copy-done), kind=kOutput, calls=%fused_computation.45 | convolution fusion | flops 805830656 | bytes 4587520 | tf_op jit(solution)/shard_map/dot_general | solution.py:80
  187.5 6.3 %all-reduce = (f32[256]{0:T(256)S(1)}, f32[256]{0:T(256)S(1)}) all-reduce(f32[256]{0:T(256)S(1)} %get-tuple-element.19, f32[256]{0:T(256)S(1)} %get-tuple-element.18), channel_id=1, replica_groups=mesh['sp'=8,'tp'=4] {'tp'}, use_global_device_ids=true, to_apply=%region_14.15 | all-reduce | flops 512 | bytes 4096 | tf_op jit(solution)/shard_map/psum | solution.py:131
  197.1 3.0 %fusion.15 = bf16[1,2048,256]{1,2,0:T(8,128)(2,1)} fusion(bf16[768,256]{1,0:T(8,128)(2,1)} %copy-done.9, bf16[1,768,2048]{2,1,0:T(8,128)(2,1)S(1)} %copy-done), kind=kOutput, calls=%fused_computation.44 | convolution fusion | flops 805830656 | bytes 4587520 | tf_op jit(solution)/shard_map/dot_general | solution.py:83
  200.1 2.3 copy.25
  202.4 2.3 copy.26
  204.7 10.9 %multiply_convert_fusion.3 = (bf16[256,512]{1,0:T(8,128)(2,1)}, f32[256,512]{1,0:T(8,128)S(1)}) fusion(bf16[256,512]{1,0:T(8,128)(2,1)} %param.24, bf16[256,512]{1,0:T(8,128)(2,1)S(1)} %copy-done.6, f32[256,512]{1,0:T(8,128)} %copy-done.2, f32[512]{0:T(512)} %bitcast.108, f32[30,512]{1,0:T(8,128)S(1)} %collective-permute-done, f32[512]{0:T(512)} %bitcast.109, ...), kind=kLoop, calls=%fused_computation.201 | loop fusion | flops 13238272 | bytes 1959936 | tf_op jit(solution)/shard_map/convert_element_type | solution.py:152
  216.4 50.7 %reduce-scatter.5.cloned.1.call-done = f32[64,2048]{1,0:T(8,128)} async-done(((f32[512,2048]{1,0:T(8,128)}), f32[64,2048]{1,0:T(8,128)}) %reduce-scatter.5.cloned.1.call-update) | async-done | bytes 524304 | tf_op jit(solution)/shard_map/reduce_scatter | solution.py:116
  (73 shorter events, 20.1 us)
Async XLA Ops:
  7.2 41.0 %copy-start = (bf16[1,768,2048]{2,1,0:T(8,128)(2,1)S(1)}, bf16[1,768,2048]{2,1,0:T(8,128)(2,1)}, u32[]{:S(2)}) copy-start(bf16[1,768,2048]{2,1,0:T(8,128)(2,1)} %param.16) | copy-start | bytes 9437188
  7.2 8.9 %copy-start.12 = (f32[256,2]{0,1:T(2,128)S(1)}, f32[256,2]{0,1:T(2,128)}, u32[]{:S(2)}) copy-start(f32[256,2]{0,1:T(2,128)} %param.15) | copy-start | bytes 6148
  7.2 68.6 %all-gather.3.cloned.1.call-start = ((), (), s32[]{:S(2)}) async-start(), calls=%async_computation.4 | async-start | bytes 3932160 | tf_op jit(solution)/shard_map/all_gather | solution.py:60
  48.1 73.9 %reduce-scatter.3.cloned.1.call-start = ((), (), s32[]{:S(2)}) async-start(), calls=%async_computation.5 | async-start | bytes 3932160 | tf_op jit(solution)/shard_map/reduce_scatter | solution.py:86
  48.1 3.2 %copy-start.4 = (bf16[1,2048,256]{2,1,0:T(8,128)(2,1)S(1)}, bf16[1,2048,256]{2,1,0:T(8,128)(2,1)}, u32[]{:S(2)}) copy-start(bf16[1,2048,256]{2,1,0:T(8,128)(2,1)} %param.17) | copy-start | bytes 3145732
  75.8 4.2 %copy-start.5 = (bf16[1,2048,256]{2,1,0:T(8,128)(2,1)S(1)}, bf16[1,2048,256]{2,1,0:T(8,128)(2,1)}, u32[]{:S(2)}) copy-start(bf16[1,2048,256]{2,1,0:T(8,128)(2,1)} %param.17) | copy-start | bytes 3145732
  79.9 1.1 copy-start.3
  79.9 1.1 copy-start.9
  79.9 1.5 copy-start.8
  122.0 25.7 %all-to-all-start.1 = ((bf16[8,96,512]{2,1,0:T(8,128)(2,1)}), bf16[8,96,512]{2,1,0:T(8,128)(2,1)}, u32[]{:S(2)}, u32[]{:S(2)}) async-start(bf16[8,96,512]{2,1,0:T(8,128)(2,1)} %bitcast.97), calls=%async_computation.2 | async-start | bytes 1572864 | tf_op jit(solution)/shard_map/all_to_all | solution.py:89
  127.5 46.8 %all-gather.5.cloned.1.call-start = ((), (), s32[]{:S(2)}) async-start(), calls=%async_computation.6 | async-start | bytes 1310720 | tf_op jit(solution)/shard_map/all_gather | solution.py:99
  151.6 7.9 %copy-start.1 = (bf16[256,512]{1,0:T(8,128)(2,1)S(1)}, bf16[256,512]{1,0:T(8,128)(2,1)}, u32[]{:S(2)}) copy-start(bf16[256,512]{1,0:T(8,128)(2,1)} %param.21) | copy-start | bytes 786436
  151.6 22.7 %copy-start.11 = (f32[512]{0:T(512)S(1)}, f32[512]{0:T(512)}, u32[]{:S(2)}) copy-start(f32[512]{0:T(512)} %param.22) | copy-start | bytes 6148
  159.5 107.6 %reduce-scatter.5.cloned.1.call-start = ((), (), s32[]{:S(2)}) async-start(), calls=%async_computation.7 | async-start | bytes 4718592 | tf_op jit(solution)/shard_map/reduce_scatter | solution.py:116
  178.4 0.8 copy-start.10
  179.2 4.4 %copy-start.13 = (bf16[8,96,2048]{2,1,0:T(8,128)(2,1)S(1)}, bf16[8,96,2048]{2,1,0:T(8,128)(2,1)}, u32[]{:S(2)}) copy-start(bf16[8,96,2048]{2,1,0:T(8,128)(2,1)} %all-gather.3.cloned.1.call-done) | copy-start | bytes 9437188
  179.2 4.4 %copy-start.15 = (f32[768,256]{1,0:T(8,128)S(1)}, f32[768,256]{1,0:T(8,128)}, u32[]{:S(2)}) copy-start(f32[768,256]{1,0:T(8,128)} %fusion.4) | copy-start | bytes 2359300
  179.3 4.4 %copy-start.16 = (f32[768,256]{1,0:T(8,128)S(1)}, f32[768,256]{1,0:T(8,128)}, u32[]{:S(2)}) copy-start(f32[768,256]{1,0:T(8,128)} %fusion.6) | copy-start | bytes 2359300
  183.7 2.2 copy-start.7
  183.7 2.2 copy-start.14
  195.0 0.8 copy-start.2
  195.8 8.8 %collective-permute-start = (f32[30,512]{1,0:T(8,128)S(1)}, f32[30,512]{1,0:T(8,128)S(1)}, u32[]{:S(2)}, u32[]{:S(2)}) collective-permute-start(f32[30,512]{1,0:T(8,128)S(1)} %slice.259), channel_id=1, source_target_pairs={{4,0},{8,4},{12,8},{16,12},{20,16},{24,20},{28,24},{5,1},{9,5},{13... | collective-permute-start | bytes 184328 | tf_op jit(solution)/shard_map/ppermute | solution.py:14
  200.1 4.6 %copy-start.6 = (bf16[256,512]{1,0:T(8,128)(2,1)S(1)}, bf16[256,512]{1,0:T(8,128)(2,1)}, u32[]{:S(2)}) copy-start(bf16[256,512]{1,0:T(8,128)(2,1)} %param.25) | copy-start | bytes 786436
Sparse Core Ops, SparseCore 0:
  48.2 27.5 all-gather.2
  84.3 37.7 reduce-scatter.2
  159.6 14.6 all-gather.4
  178.6 88.4 reduce-scatter.4
where the time goes:
time: 274 us
  waiting for transfers between devices  140 us (51%)
  blocking collectives  39.7 us (14%)
  matrix products  26.9 us (10%)
  other arithmetic  24.5 us (9%)
  local copies, waits for them, and re-layouts  21.7 us (8%)
  between operations  14 us (5%)
  starting transfers between devices  7.13 us (3%)
    reduce_scatter x1, waiting for transfers between devices, per_device(): lax.psum_scatter(lax.dot_general(act_conv, mix_full, (((0,), (0,)), ((),...  50.7 us
    reduce_scatter x1, waiting for transfers between devices, per_device(): lax.psum_scatter(partial_value.astype(jnp.bfloat16), 'tp', scatter_dimens...  37.9 us
    all_to_all x1, blocking collectives, per_device(): lax.all_to_all(outgoing.reshape(group_size, capacity, local_cols), 'sp',...  27.5 us
    all_gather x1, waiting for transfers between devices, per_device(): arrived = lax.all_gather(moved, 'tp', axis=2, tiled=True)  22.5 us
    all_to_all x1, waiting for transfers between devices, per_device(): lax.all_to_all(input_grad.reshape(group_size, capacity, local_cols), 'sp'...  19.9 us
    convert_element_type x1, other arithmetic, per_device(): (d_glu * value_pre.astype(jnp.float32) * gate_sig * (1.0 - gate_sig)).ast...  10.9 us
    all_gather x1, waiting for transfers between devices, per_device(): mix_full = lax.all_gather(mix_grad, 'tp', axis=1, tiled=True)  8.69 us
    unnamed x38, local copies, waits for them, and re-layouts  7.74 us
  transfers between devices with their start and end apart: 6, of which 5 were waited for; matrix products, arithmetic and copies ran while one was open for 12% of the time, Pallas kernels for 0%

commit v1 on v0

v1 whole, which is shorter than its diff:
```python
import functools

import jax
import jax.numpy as jnp
from jax import lax
from jax.experimental import pallas as pl
from jax.experimental.pallas import tpu as pltpu
from jax.sharding import PartitionSpec as P

clamp_limit = 7.0
swish_alpha = 1.702
norm_epsilon = 1e-05
MESH = pl.DeviceIdType.MESH
VMEM = pltpu.VMEM


def passed_along(value, axis, steps):
    count = lax.axis_size(axis)
    leading, last = (max(0, -steps), min(count, count - steps))
    return lax.ppermute(value, axis, [(source, source + steps) for source in range(leading, last)])


def lanes(index, width):
    return pl.ds(pl.multiple_of(index * width, width), width)


def places(group, narrow):
    me, t = lax.axis_index("sp"), lax.axis_index("tp")
    near = t + 1 - 2 * lax.rem(t, 2)
    far = lax.rem(t + narrow // 2, narrow)
    return me, t, near, far, lax.rem(near + narrow // 2, narrow)


def remote(src, dst, send, recv, sp, tp):
    return pltpu.make_async_remote_copy(
        src_ref=src, dst_ref=dst, send_sem=send, recv_sem=recv, device_id=(sp, tp), device_id_type=MESH
    )


def meet(peers):
    barrier = pltpu.get_barrier_semaphore()
    for sp, tp in peers:
        pl.semaphore_signal(barrier, inc=1, device_id=(sp, tp), device_id_type=MESH)
    pl.semaphore_wait(barrier, len(peers))


def dispatch_kernel(group, narrow, width, out_ref, stat_ref, rows_ref, stats_ref, *sems):
    a_s, a_r, n_s, n_r, f_s, f_r, m_s, m_r, t_s, t_r, l_s = sems
    me, t, near, far, cross = places(group, narrow)
    sp_peers = [lax.rem(me + o, group) for o in range(1, group)]
    meet([(p, t) for p in sp_peers] + [(me, near), (me, far), (me, cross)])

    def spot(s, column):
        return rows_ref.at[s, :, lanes(column, width)]

    def swap(s):
        return remote(out_ref.at[s], spot(me, t), a_s.at[s], a_r.at[me], s, t)

    for p in sp_peers:
        swap(p).start()
    stat_own = pltpu.make_async_copy(stat_ref, stats_ref.at[t], l_s.at[0])
    stat_own.start()
    small = []
    for k, p in enumerate((near, far, cross)):
        c = remote(stat_ref, stats_ref.at[t], t_s.at[k], t_r.at[k], me, p)
        c.start()
        small.append(c)
    own = pltpu.make_async_copy(out_ref.at[me], spot(me, t), l_s.at[1])
    own.start()
    own.wait()
    order = [me] + [lax.rem(me + group - o, group) for o in range(1, group)]

    def to_far(s):
        return remote(spot(s, t), spot(s, t), f_s.at[s], f_r.at[s], me, far)

    def to_near(s):
        return remote(spot(s, t), spot(s, t), n_s.at[s], n_r.at[s], me, near)

    def onward(s):
        return remote(spot(s, far), spot(s, far), m_s.at[s], m_r.at[s], me, near)

    for i, s in enumerate(order):
        if i > 0:
            remote(out_ref.at[s], spot(s, t), a_s.at[s], a_r.at[s], s, t).wait_recv()
        to_far(s).start()
        to_near(s).start()
        if i > 0:
            prev = order[i - 1]
            remote(spot(prev, far), spot(prev, far), f_s.at[prev], f_r.at[prev], me, far).wait_recv()
            onward(prev).start()
    last = order[-1]
    remote(spot(last, far), spot(last, far), f_s.at[last], f_r.at[last], me, far).wait_recv()
    onward(last).start()
    for s in order:
        to_far(s).wait_send()
        to_near(s).wait_send()
        onward(s).wait_send()
        remote(spot(s, near), spot(s, near), n_s.at[s], n_r.at[s], me, near).wait_recv()
        remote(spot(s, cross), spot(s, cross), m_s.at[s], m_r.at[s], me, near).wait_recv()
    for p in sp_peers:
        swap(p).wait_send()
    stat_own.wait()
    for c in small:
        c.wait_send()
        c.wait_recv()


def dispatch(outgoing, stat):
    group, capacity, width = outgoing.shape
    narrow = lax.axis_size("tp")
    dma = pltpu.SemaphoreType.DMA
    return pl.pallas_call(
        functools.partial(dispatch_kernel, group, narrow, width),
        out_shape=(
            jax.ShapeDtypeStruct((group, capacity, narrow * width), outgoing.dtype),
            jax.ShapeDtypeStruct((narrow,) + stat.shape, stat.dtype),
        ),
        in_specs=[pl.BlockSpec(memory_space=VMEM)] * 2,
        out_specs=[pl.BlockSpec(memory_space=VMEM)] * 2,
        scratch_shapes=[dma((group,))] * 8 + [dma((3,))] * 2 + [dma((2,))],
        compiler_params=pltpu.CompilerParams(collective_id=0, has_side_effects=True),
    )(outgoing, stat)


def return_kernel(group, narrow, width, part_ref, home_ref, pair_buf, far_out, far_in, done, *sems):
    n_s, n_r, f_s, f_r, a_s, a_r, l_s = sems
    me, t, near, far, cross = places(group, narrow)
    sp_peers = [lax.rem(me + o, group) for o in range(1, group)]
    meet([(p, t) for p in sp_peers] + [(me, near), (me, far)])
    order = sp_peers + [me]

    def part(s, column):
        return part_ref.at[s, :, lanes(column, width)]

    def to_near(s, k):
        return remote(
            part(s, near if k == 0 else cross), pair_buf.at[s, k], n_s.at[s, k], n_r.at[s, k], me, near
        )

    def to_far(s):
        return remote(far_out.at[s], far_in.at[s], f_s.at[s], f_r.at[s], me, far)

    def to_home(s):
        return remote(done.at[s], home_ref.at[me], a_s.at[s], a_r.at[me], s, t)

    for s in order:
        to_near(s, 1).start()
        to_near(s, 0).start()
    own = pltpu.make_async_copy(done.at[me], home_ref.at[me], l_s.at[0])

    def finish(s, i):
        to_near(s, 0).wait_recv()
        to_far(s).wait_recv()
        total = part_ref[s, :, lanes(t, width)].astype(jnp.float32)
        total = total + pair_buf[s, 0].astype(jnp.float32) + far_in[s].astype(jnp.float32)
        done[s] = total.astype(done.dtype)
        if i < group - 1:
            to_home(s).start()
        else:
            own.start()

    lag = min(2, group - 1)
    for i, s in enumerate(order):
        to_near(s, 1).wait_recv()
        pair = part_ref[s, :, lanes(far, width)].astype(jnp.float32) + pair_buf[s, 1].astype(jnp.float32)
        far_out[s] = pair.astype(far_out.dtype)
        to_far(s).start()
        if i >= lag:
            finish(order[i - lag], i - lag)
    for i in range(group - lag, group):
        finish(order[i], i)
    own.wait()
    for s in order:
        to_near(s, 0).wait_send()
        to_near(s, 1).wait_send()
        to_far(s).wait_send()
    for s in sp_peers:
        to_home(s).wait_send()
        remote(done.at[s], home_ref.at[s], a_s.at[s], a_r.at[s], s, t).wait_recv()


def return_home(partial):
    group, capacity, whole = partial.shape
    narrow = lax.axis_size("tp")
    width = whole // narrow
    dma = pltpu.SemaphoreType.DMA
    block = (group, capacity, width)
    return pl.pallas_call(
        functools.partial(return_kernel, group, narrow, width),
        out_shape=jax.ShapeDtypeStruct(block, partial.dtype),
        in_specs=[pl.BlockSpec(memory_space=VMEM)],
        out_specs=pl.BlockSpec(memory_space=VMEM),
        scratch_shapes=[
            VMEM((group, 2, capacity, width), partial.dtype),
            VMEM(block, partial.dtype),
            VMEM(block, partial.dtype),
            VMEM(block, partial.dtype),
        ]
        + [dma((group, 2))] * 2
        + [dma((group,))] * 4
        + [dma((1,))],
        compiler_params=pltpu.CompilerParams(collective_id=1, has_side_effects=True),
    )(partial)


def widen_kernel(narrow, width, pieces, mix_ref, full_ref, *sems):
    n_s, n_r, f_s, f_r, m_s, m_r, l_s = sems
    me, t, near, far, cross = places(1, narrow)
    meet([(me, near), (me, far)])
    rows = mix_ref.shape[0] // pieces

    def src(k):
        return mix_ref.at[pl.ds(k * rows, rows)]

    def spot(k, column):
        return full_ref.at[pl.ds(k * rows, rows), lanes(column, width)]

    def to_far(k):
        return remote(src(k), spot(k, t), f_s.at[k], f_r.at[k], me, far)

    def to_near(k):
        return remote(src(k), spot(k, t), n_s.at[k], n_r.at[k], me, near)

    def onward(k):
        return remote(spot(k, far), spot(k, far), m_s.at[k], m_r.at[k], me, near)

    own = pltpu.make_async_copy(mix_ref, full_ref.at[:, lanes(t, width)], l_s.at[0])
    for k in range(pieces):
        to_far(k).start()
    for k in range(pieces):
        to_near(k).start()
    own.start()
    for k in range(pieces):
        to_far(k).wait_recv()
        onward(k).start()
    own.wait()
    for k in range(pieces):
        to_far(k).wait_send()
        to_near(k).wait()
        onward(k).wait()


def widen(mix):
    rows, width = mix.shape
    narrow = lax.axis_size("tp")
    pieces = 4
    dma = pltpu.SemaphoreType.DMA
    return pl.pallas_call(
        functools.partial(widen_kernel, narrow, width, pieces),
        out_shape=jax.ShapeDtypeStruct((rows, narrow * width), mix.dtype),
        in_specs=[pl.BlockSpec(memory_space=VMEM)],
        out_specs=pl.BlockSpec(memory_space=VMEM),
        scratch_shapes=[dma((pieces,))] * 6 + [dma((1,))],
        compiler_params=pltpu.CompilerParams(collective_id=2, has_side_effects=True),
    )(mix)


def per_device(
    cot_out,
    route_ids,
    route_weight,
    expert_inputs,
    w_gate,
    w_up,
    w_down,
    w_proj,
    conv_out,
    channel_norm_gain,
    taps,
    value_pre,
    gate_pre,
):
    group_size = lax.axis_size("sp")
    narrow_size = lax.axis_size("tp")
    tok_rows, local_cols = cot_out.shape
    chosen = route_ids.shape[1]
    slot_rows = expert_inputs.shape[1]
    capacity = slot_rows // group_size
    model_width = expert_inputs.shape[2]
    f32, bf16 = jnp.float32, jnp.bfloat16
    experts = jnp.arange(group_size, dtype=jnp.int32)[None, :]
    hots = [(route_ids[:, k : k + 1] == experts) for k in range(chosen)]
    hot = functools.reduce(jnp.logical_or, hots)
    token = jnp.arange(tok_rows, dtype=jnp.int32)
    before = (token[:, None] > token[None, :]).astype(bf16)
    earlier = jnp.dot(before, hot.astype(bf16), preferred_element_type=f32)
    slots = jnp.arange(slot_rows, dtype=jnp.int32)[None, :]
    picks, scaled = [], []
    for k in range(chosen):
        slot = jnp.sum(jnp.where(hots[k], earlier, 0.0), axis=1).astype(jnp.int32)
        dest = route_ids[:, k] * capacity + slot
        picks.append((dest[:, None] == slots).astype(bf16))
        scaled.append((route_weight[:, k : k + 1] * cot_out.astype(f32)).astype(bf16))
    outgoing = lax.dot_general(
        jnp.concatenate(picks, axis=0),
        jnp.concatenate(scaled, axis=0),
        (((0,), (0,)), ((), ())),
        preferred_element_type=f32,
    ).astype(bf16)
    convolution_filter = conv_out.astype(f32)
    stat = jnp.stack(
        [jnp.sum(convolution_filter, axis=1), jnp.sum(convolution_filter * convolution_filter, axis=1)]
    )
    arrived, stats = dispatch(outgoing.reshape(group_size, capacity, local_cols), stat)
    rows_cot = arrived.reshape(slot_rows, model_width)
    rows_in = expert_inputs[0]
    gate_weight = w_gate[0]
    up_weight = w_up[0]
    down_weight = w_down[0]
    gate_lin = jnp.dot(rows_in, gate_weight, preferred_element_type=f32)
    up_lin = jnp.dot(rows_in, up_weight, preferred_element_type=f32)
    gate_c = jnp.minimum(gate_lin, clamp_limit)
    up_c = jnp.clip(up_lin, -clamp_limit, clamp_limit)
    sigma = jax.nn.sigmoid(swish_alpha * gate_c)
    act = ((up_c + 1.0) * gate_c * sigma).astype(bf16)
    grad_down = jnp.dot(act.T, rows_cot, preferred_element_type=f32).astype(bf16)
    d_act = jnp.dot(rows_cot, down_weight.T, preferred_element_type=f32)
    up_open = ((up_lin > -clamp_limit) & (up_lin < clamp_limit)).astype(f32)
    gate_open = (gate_lin < clamp_limit).astype(f32)
    d_up = (d_act * gate_c * sigma * up_open).astype(bf16)
    d_gate = (
        d_act * (up_c + 1.0) * (sigma + swish_alpha * gate_c * sigma * (1.0 - sigma)) * gate_open
    ).astype(bf16)
    grad_gate_part = jnp.dot(rows_in.T, d_gate, preferred_element_type=f32).astype(bf16)
    grad_up_part = jnp.dot(rows_in.T, d_up, preferred_element_type=f32).astype(bf16)
    partial_value = jnp.dot(d_gate, gate_weight.T, preferred_element_type=f32)
    partial_value = partial_value + jnp.dot(d_up, up_weight.T, preferred_element_type=f32)
    coming = return_home(partial_value.astype(bf16).reshape(group_size, capacity, model_width))
    pick_any = functools.reduce(jnp.add, picks)
    summed = jnp.dot(pick_any, coming.reshape(slot_rows, local_cols), preferred_element_type=f32)
    mix_grad = (cot_out.astype(f32) + summed).astype(bf16)
    mix_full = widen(mix_grad)
    channel_total = local_cols * narrow_size
    first_sum, square_sum = jnp.sum(stats, axis=0)
    channel_mean = (first_sum / channel_total)[:, None]
    var = (square_sum / channel_total)[:, None] - channel_mean * channel_mean
    inverse_deviation = lax.rsqrt(var + norm_epsilon)
    normalized_input = (convolution_filter - channel_mean) * inverse_deviation
    normalized_output = normalized_input * channel_norm_gain[None, :]
    sigma_conv = jax.nn.sigmoid(normalized_output)
    act_conv = (normalized_output * sigma_conv).astype(bf16)
    grad_proj = lax.psum_scatter(
        lax.dot_general(act_conv, mix_full, (((0,), (0,)), ((), ())), preferred_element_type=f32).astype(
            bf16
        ),
        "sp",
        scatter_dimension=0,
        tiled=True,
    ).astype(f32)
    d_act_conv = jnp.dot(mix_full, w_proj.T, preferred_element_type=f32)
    normalized_gradient = (
        d_act_conv
        * sigma_conv
        * (1.0 + normalized_output * (1.0 - sigma_conv))
        * channel_norm_gain[None, :]
    )
    first_term_gradient, second_term_gradient = lax.psum(
        (
            jnp.sum(normalized_gradient, axis=1),
            jnp.sum(normalized_gradient * normalized_input, axis=1),
        ),
        "tp",
    )
    convolution_gradient = inverse_deviation * (
        normalized_gradient
        - (first_term_gradient / channel_total)[:, None]
        - normalized_input * (second_term_gradient / channel_total)[:, None]
    )
    reach = taps.shape[0]
    following = passed_along(convolution_gradient[: reach - 1], "sp", -1)
    extended = jnp.concatenate([convolution_gradient, following], axis=0)
    d_glu = jnp.zeros_like(convolution_gradient)
    for offset in range(reach):
        begin = reach - 1 - offset
        d_glu = d_glu + taps[offset][None, :] * extended[begin : begin + tok_rows]
    gate_sig = jax.nn.sigmoid(gate_pre.astype(f32))
    grad_value = (d_glu * gate_sig).astype(bf16)
    grad_gate = (d_glu * value_pre.astype(f32) * gate_sig * (1.0 - gate_sig)).astype(bf16)
    return (
        grad_gate_part[None],
        grad_up_part[None],
        grad_down[None],
        grad_proj,
        grad_value,
        grad_gate,
    )


def solution(mesh):
    return jax.shard_map(
        per_device,
        mesh=mesh,
        in_specs=(
            P("sp", "tp"),
            P("sp", None),
            P("sp", None),
            P("sp", None, None),
            P("sp", None, "tp"),
            P("sp", None, "tp"),
            P("sp", "tp", None),
            P("tp", None),
            P("sp", "tp"),
            P("tp"),
            P(None, "tp"),
            P("sp", "tp"),
            P("sp", "tp"),
        ),
        out_specs=(
            P("sp", None, "tp"),
            P("sp", None, "tp"),
            P("sp", "tp", None),
            P(("tp", "sp"), None),
            P("sp", "tp"),
            P("sp", "tp"),
        ),
        check_vma=False,
    )
```

time: 274 us -> 191 us (0.70)
  waiting for transfers between devices: 140 us -> 25.9 us
  Pallas kernels: 0 us -> 80.8 us
  blocking collectives: 39.7 us -> 7.03 us
  local copies, waits for them, and re-layouts: 21.7 us -> 11.8 us
  starting transfers between devices: 7.13 us -> 1.5 us
  other arithmetic: 24.5 us -> 19.1 us
  matrix products: 26.9 us -> 30.1 us
    pallas_call x0 -> x3, Pallas kernels: none -> 80.8 us  [the longest x1 35.3 us: dispatch(): pl.pallas_call(functools.partial(dispatch_kernel, group, narrow, width),...]
    reduce_scatter x1 -> x0, waiting for transfers between devices: 37.9 us -> none  [per_device(): lax.psum_scatter(partial_value.astype(jnp.bfloat16), 'tp', scatter_dimens...]
    all_gather x2 -> x0, waiting for transfers between devices: 31.2 us -> none  [the longest x1 22.5 us: per_device(): arrived = lax.all_gather(moved, 'tp', axis=2, tiled=True)]
    all_to_all x1 -> x0, blocking collectives: 27.5 us -> none  [per_device(): lax.all_to_all(outgoing.reshape(group_size, capacity, local_cols), 'sp',...]
    reduce_scatter x1, waiting for transfers between devices: 50.7 us -> 25.8 us  [per_device(): lax.psum_scatter(lax.dot_general(act_conv, mix_full, (((0,), (0,)), ((),...]
    all_to_all x1 -> x0, waiting for transfers between devices: 19.9 us -> none  [per_device(): lax.all_to_all(input_grad.reshape(group_size, capacity, local_cols), 'sp'...]
    psum x1 -> x0, blocking collectives: 5.91 us -> none  [per_device(): lax.psum((jnp.sum(convolution_filter, axis=1), jnp.sum(convolution_filter...]
    convert_element_type x2 -> x0, local copies, waits for them, and re-layouts: 5.62 us -> none  [the longest x1 2.91 us: per_device(): jnp.repeat(cot_out, chosen, axis=0).astype(jnp.float32)]
  transfers between devices with their start and end apart: 6 -> 2, of which waited for: 5 -> 1; matrix products, arithmetic and copies ran while one was open for 12% -> 18% of each run, Pallas kernels for 0% -> 0%
where the time goes in v1:
time: 191 us
  Pallas kernels  80.8 us (42%)
  matrix products  30.1 us (16%)
  waiting for transfers between devices  25.9 us (14%)
  other arithmetic  19.1 us (10%)
  between operations  14.5 us (8%)
  local copies, waits for them, and re-layouts  11.8 us (6%)
  blocking collectives  7.03 us (4%)
    pallas_call x1, Pallas kernels, dispatch(): pl.pallas_call(functools.partial(dispatch_kernel, group, narrow, width),...  35.3 us
    pallas_call x1, Pallas kernels, return_home(): pl.pallas_call(functools.partial(return_kernel, group, narrow, width), ou...  34.3 us
    reduce_scatter x1, waiting for transfers between devices, per_device(): lax.psum_scatter(lax.dot_general(act_conv, mix_full, (((0,), (0,)), ((),...  25.8 us
    convert_element_type x1, other arithmetic, per_device(): (d_glu * value_pre.astype(f32) * gate_sig * (1.0 - gate_sig)).astype(bf16)  12.6 us
    pallas_call x1, Pallas kernels, widen(): pl.pallas_call(functools.partial(widen_kernel, narrow, width, pieces), ou...  11.2 us
    unnamed x64, local copies, waits for them, and re-layouts  8.38 us
    psum x1, blocking collectives, per_device(): lax.psum((jnp.sum(normalized_gradient, axis=1), jnp.sum(normalized_gradie...  7.03 us
    dot_general x1, matrix products, per_device(): d_act = jnp.dot(rows_cot, down_weight.T, preferred_element_type=f32)  4.14 us
  transfers between devices with their start and end apart: 2, of which 1 were waited for; matrix products, arithmetic and copies ran while one was open for 18% of the time, Pallas kernels for 0%

profile of v1, /device:TPU:0, one launch (start us, length us, event | category | flops | bytes accessed | tf_op | source)
XLA Modules:
  0.0 190.7 jit_solution(2567699679457704782)
XLA Ops:
  7.2 1.8 copy-done
  9.1 3.2 %fusion.4 = f32[768,256]{1,0:T(8,128)} fusion(bf16[1,768,2048]{2,1,0:T(8,128)(2,1)S(1)} %copy-done, bf16[1,2048,256]{2,1,0:T(8,128)(2,1)} %param.18), kind=kOutput, calls=%fused_computation.34 | convolution fusion | flops 805306368 | bytes 4980736 | tf_op jit(solution)/shard_map/dot_general | solution.py:311
  12.3 1.9 fusion.6
  15.5 1.5 convolution_convert_fusion.2
  17.0 35.3 %shard_map.172 = (bf16[8,96,2048]{2,1,0:T(8,128)(2,1)}, f32[4,2,256]{2,1,0:T(2,128)}) custom-call(bf16[8,96,512]{2,1,0:T(8,128)(2,1)} %bitcast.100, f32[2,256]{1,0:T(2,128)} %pad_maximum_fusion.1.stat_ref), custom_call_target="tpu_custom_call" | custom-call | tf_op jit(solution)/shard_map/pallas_call | solution.py:112
  52.4 4.1 %select_convert_fusion = (bf16[768,256]{1,0:T(8,128)(2,1)S(1)}, bf16[768,256]{1,0:T(8,128)(2,1)S(1)}) fusion(f32[768,256]{1,0:T(8,128)} %fusion.4, f32[768,256]{1,0:T(8,128)} %fusion.6, bf16[768,2048]{1,0:T(8,128)(2,1)} %bitcast.150, bf16[1,256,2048]{2,1,0:T(8,128)(2,1)} %param.19), kind=kOutput, calls=%fused_computation.62 | convolution fusion | flops 809828352 | bytes 6553600 | tf_op jit(solution)/shard_map/dot_general | solution.py:317
  57.9 2.7 %add_convert_fusion = bf16[768,2048]{1,0:T(8,128)(2,1)} fusion(f32[768,2048]{1,0:T(8,128)S(1)} %fusion.28, bf16[768,256]{1,0:T(8,128)(2,1)S(1)} %get-tuple-element.26, bf16[1,2048,256]{2,1,0:T(8,128)(2,1)S(1)} %copy-done.6), kind=kOutput, calls=%fused_computation.29 | convolution fusion | flops 808452096 | bytes 10878976 | tf_op jit(solution)/shard_map/dot_general | solution.py:327
  60.6 34.3 %shard_map.173 = bf16[8,96,512]{2,1,0:T(8,128)(2,1)} custom-call(bf16[8,96,2048]{2,1,0:T(8,128)(2,1)} %bitcast.99), custom_call_target="tpu_custom_call" | custom-call | tf_op jit(solution)/shard_map/pallas_call | solution.py:188
  94.9 2.3 %fusion.23.mix_ref = bf16[256,512]{1,0:T(8,128)(2,1)} fusion(bf16[768,512]{1,0:T(8,128)(2,1)} %bitcast.101, bf16[256,512]{1,0:T(8,128)(2,1)} %param.13, s32[256]{0:T(256)S(1)} %bitcast.140, s32[256]{0:T(256)S(1)} %bitcast.138), kind=kOutput, calls=%fused_computation.50 | convolution fusion | flops 203292672 | bytes 1312768 | tf_op jit(solution)/shard_map/dot_general | solution.py:330
  97.2 11.2 %shard_map.174 = bf16[256,2048]{1,0:T(8,128)(2,1)} custom-call(bf16[256,512]{1,0:T(8,128)(2,1)} %fusion.23.mix_ref), custom_call_target="tpu_custom_call" | custom-call | tf_op jit(solution)/shard_map/pallas_call | solution.py:248
  108.4 3.6 %convolution_convert_fusion = bf16[512,2048]{1,0:T(8,128)(2,1)} fusion(bf16[256,2048]{1,0:T(8,128)(2,1)} %shard_map.174, bf16[256,512]{1,0:T(8,128)(2,1)} %param.21, f32[512]{0:T(512)} %param.22, f32[256]{0:T(256)S(1)} %add_rsqrt_fusion, f32[256]{0:T(256)S(1)} %bitcast.103), kind=kOutput, calls=%fused_computation.38 | convolution fusion | flops 539099136 | bytes 3411968 | tf_op jit(solution)/shard_map/dot_general | solution.py:343
  112.1 3.6 %fusion.169 = (f32[256]{0:T(256)S(1)}, f32[256]{0:T(256)S(1)}, f32[256,512]{1,0:T(8,128)}) fusion(f32[256]{0:T(256)S(1)} %add_rsqrt_fusion, f32[256]{0:T(256)S(1)} %bitcast.104, bf16[256,512]{1,0:T(8,128)(2,1)} %param.21, f32[512]{0:T(512)} %param.22, bf16[256,2048]{1,0:T(8,128)(2,1)} %shard_map.174, bf16[512,2048]{1,0:T(8,128)(2,1)} %param.20), kind=kOutput, calls=%fused_computation.250 | convolution fusion | flops 538967552 | bytes 3938304 | tf_op jit(solution)/shard_map/dot_general | solution.py:350
  115.7 7.0 %all-reduce = (f32[256]{0:T(256)}, f32[256]{0:T(256)}) all-reduce(f32[256]{0:T(256)S(1)} %get-tuple-element.17, f32[256]{0:T(256)S(1)} %get-tuple-element.16), channel_id=1, replica_groups=mesh['sp'=8,'tp'=4] {'tp'}, use_global_device_ids=true, to_apply=%region_9.10 | all-reduce | flops 512 | bytes 4096 | tf_op jit(solution)/shard_map/psum | solution.py:357
  124.0 1.4 fusion.141
  126.9 1.5 collective-permute-start
  128.3 1.8 fusion.171
  130.1 2.0 %fusion.18 = bf16[1,2048,256]{1,2,0:T(8,128)(2,1)} fusion(bf16[768,256]{1,0:T(8,128)(2,1)S(1)} %get-tuple-element.27, bf16[1,768,2048]{2,1,0:T(8,128)(2,1)S(1)} %copy-done), kind=kOutput, calls=%fused_computation.44 | convolution fusion | flops 805830656 | bytes 4587520 | tf_op jit(solution)/shard_map/dot_general | solution.py:324
  132.1 2.0 %fusion.15 = bf16[1,2048,256]{1,2,0:T(8,128)(2,1)} fusion(bf16[768,256]{1,0:T(8,128)(2,1)S(1)} %copy-done.8, bf16[1,768,2048]{2,1,0:T(8,128)(2,1)S(1)} %copy-done), kind=kOutput, calls=%fused_computation.43 | convolution fusion | flops 805830656 | bytes 4587520 | tf_op jit(solution)/shard_map/dot_general | solution.py:325
  134.9 2.1 %fusion.14 = bf16[1,256,2048]{2,1,0:T(8,128)(2,1)} fusion(bf16[768,2048]{1,0:T(8,128)(2,1)S(1)} %bitcast.151, f32[768,256]{1,0:T(8,128)S(1)} %copy-done.30, f32[768,256]{1,0:T(8,128)S(1)} %copy-done.29), kind=kOutput, calls=%fused_computation.42 | convolution fusion | flops 807796736 | bytes 5767168 | tf_op jit(solution)/shard_map/dot_general | solution.py:316
  138.2 2.3 %copy.19 = bf16[1,2048,256]{2,1,0:T(8,128)(2,1)} copy(bf16[1,2048,256]{1,2,0:T(8,128)(2,1)} %fusion.18) | data formatting | bytes 2097152
  140.4 2.3 %copy.20 = bf16[1,2048,256]{2,1,0:T(8,128)(2,1)} copy(bf16[1,2048,256]{1,2,0:T(8,128)(2,1)} %fusion.15) | data formatting | bytes 2097152
  142.8 12.6 %multiply_convert_fusion.1 = (bf16[256,512]{1,0:T(8,128)(2,1)}, f32[256,512]{1,0:T(8,128)S(1)}) fusion(bf16[256,512]{1,0:T(8,128)(2,1)} %param.24, bf16[256,512]{1,0:T(8,128)(2,1)S(1)} %copy-done.5, f32[256,512]{1,0:T(8,128)} %copy-done.1, f32[512]{0:T(512)S(1)} %bitcast.135, f32[30,512]{1,0:T(8,128)} %collective-permute-done, f32[512]{0:T(512)S(1)} %bitcast.136, ...), kind=kLoop, calls=%fused_computation.215 | loop fusion | flops 13238272 | bytes 1959936 | tf_op jit(solution)/shard_map/convert_element_type | solution.py:378
  156.3 25.8 %reduce-scatter.2.cloned.1.call-done = bf16[64,2048]{1,0:T(8,128)(2,1)} async-done(((bf16[512,2048]{1,0:T(8,128)(2,1)}), bf16[64,2048]{1,0:T(8,128)(2,1)}) %reduce-scatter.2.cloned.1.call-update) | async-done | bytes 262160 | tf_op jit(solution)/shard_map/reduce_scatter | solution.py:342
  182.1 1.8 convert_element_type.127
  (83 shorter events, 8.3 us)
Async XLA Ops:
  7.2 174.9 %reduce-scatter.2.cloned.1.call-start = ((), (), s32[]{:S(2)}) async-start(), calls=%async_computation.1 | async-start | bytes 2359296 | tf_op jit(solution)/shard_map/reduce_scatter | solution.py:342
  9.1 3.2 %copy-start.2 = (bf16[1,2048,256]{2,1,0:T(8,128)(2,1)S(1)}, bf16[1,2048,256]{2,1,0:T(8,128)(2,1)}, u32[]{:S(2)}) copy-start(bf16[1,2048,256]{2,1,0:T(8,128)(2,1)} %param.17) | copy-start | bytes 3145732
  12.3 3.1 %copy-start.9 = (bf16[256,512]{1,0:T(8,128)(2,1)S(1)}, bf16[256,512]{1,0:T(8,128)(2,1)}, u32[]{:S(2)}) copy-start(bf16[256,512]{1,0:T(8,128)(2,1)} %param.13) | copy-start | bytes 786436
  52.3 4.2 %copy-start.3 = (bf16[1,2048,256]{2,1,0:T(8,128)(2,1)S(1)}, bf16[1,2048,256]{2,1,0:T(8,128)(2,1)}, u32[]{:S(2)}) copy-start(bf16[1,2048,256]{2,1,0:T(8,128)(2,1)} %param.17) | copy-start | bytes 3145732
  60.6 47.8 %copy-start.26 = (f32[4,2,256]{2,1,0:T(2,128)S(1)}, f32[4,2,256]{2,1,0:T(2,128)}, u32[]{:S(2)}) copy-start(f32[4,2,256]{2,1,0:T(2,128)} %get-tuple-element.9) | copy-start | bytes 24580
  124.0 8.0 %copy-start.8 = (bf16[768,256]{1,0:T(8,128)(2,1)S(1)}, bf16[768,256]{1,0:T(8,128)(2,1)}, u32[]{:S(2)}) copy-start(bf16[768,256]{1,0:T(8,128)(2,1)} %copy-done.7) | copy-start | bytes 1179652
  126.9 15.8 %collective-permute-start = (f32[30,512]{1,0:T(8,128)}, f32[30,512]{1,0:T(8,128)}, u32[]{:S(2)}, u32[]{:S(2)}) collective-permute-start(f32[30,512]{1,0:T(8,128)} %slice.266), channel_id=1, source_target_pairs={{4,0},{8,4},{12,8},{16,12},{20,16},{24,20},{28,24},{5,1},{9,5},{13... | collective-permute-start | bytes 184328 | tf_op jit(solution)/shard_map/ppermute | solution.py:20
  132.1 2.8 %copy-start.30 = (f32[768,256]{1,0:T(8,128)S(1)}, f32[768,256]{1,0:T(8,128)}, u32[]{:S(2)}) copy-start(f32[768,256]{1,0:T(8,128)} %fusion.6) | copy-start | bytes 2359300
  137.0 5.7 %copy-start.5 = (bf16[256,512]{1,0:T(8,128)(2,1)S(1)}, bf16[256,512]{1,0:T(8,128)(2,1)}, u32[]{:S(2)}) copy-start(bf16[256,512]{1,0:T(8,128)(2,1)} %param.25) | copy-start | bytes 786436
  137.0 5.7 %copy-start.10 = (f32[1,512]{1,0:T(1,128)S(1)}, f32[1,512]{1,0:T(1,128)}, u32[]{:S(2)}) copy-start(f32[1,512]{1,0:T(1,128)} %get-tuple-element.34) | copy-start | bytes 6148
  137.0 5.7 %copy-start.11 = (f32[1,512]{1,0:T(1,128)S(1)}, f32[1,512]{1,0:T(1,128)}, u32[]{:S(2)}) copy-start(f32[1,512]{1,0:T(1,128)} %get-tuple-element.35) | copy-start | bytes 6148
  137.0 5.7 %copy-start.12 = (f32[1,512]{1,0:T(1,128)S(1)}, f32[1,512]{1,0:T(1,128)}, u32[]{:S(2)}) copy-start(f32[1,512]{1,0:T(1,128)} %get-tuple-element.36) | copy-start | bytes 6148
  137.0 5.7 %copy-start.13 = (f32[1,512]{1,0:T(1,128)S(1)}, f32[1,512]{1,0:T(1,128)}, u32[]{:S(2)}) copy-start(f32[1,512]{1,0:T(1,128)} %get-tuple-element.37) | copy-start | bytes 6148
  137.0 5.7 %copy-start.14 = (f32[1,512]{1,0:T(1,128)S(1)}, f32[1,512]{1,0:T(1,128)}, u32[]{:S(2)}) copy-start(f32[1,512]{1,0:T(1,128)} %get-tuple-element.38) | copy-start | bytes 6148
  137.1 5.7 %copy-start.15 = (f32[1,512]{1,0:T(1,128)S(1)}, f32[1,512]{1,0:T(1,128)}, u32[]{:S(2)}) copy-start(f32[1,512]{1,0:T(1,128)} %get-tuple-element.39) | copy-start | bytes 6148
  137.1 5.7 %copy-start.16 = (f32[1,512]{1,0:T(1,128)S(1)}, f32[1,512]{1,0:T(1,128)}, u32[]{:S(2)}) copy-start(f32[1,512]{1,0:T(1,128)} %get-tuple-element.40) | copy-start | bytes 6148
  137.1 5.7 %copy-start.17 = (f32[1,512]{1,0:T(1,128)S(1)}, f32[1,512]{1,0:T(1,128)}, u32[]{:S(2)}) copy-start(f32[1,512]{1,0:T(1,128)} %get-tuple-element.41) | copy-start | bytes 6148
  137.1 5.7 %copy-start.18 = (f32[1,512]{1,0:T(1,128)S(1)}, f32[1,512]{1,0:T(1,128)}, u32[]{:S(2)}) copy-start(f32[1,512]{1,0:T(1,128)} %get-tuple-element.42) | copy-start | bytes 6148
  137.1 5.7 %copy-start.19 = (f32[1,512]{1,0:T(1,128)S(1)}, f32[1,512]{1,0:T(1,128)}, u32[]{:S(2)}) copy-start(f32[1,512]{1,0:T(1,128)} %get-tuple-element.43) | copy-start | bytes 6148
  137.1 5.7 %copy-start.20 = (f32[1,512]{1,0:T(1,128)S(1)}, f32[1,512]{1,0:T(1,128)}, u32[]{:S(2)}) copy-start(f32[1,512]{1,0:T(1,128)} %get-tuple-element.44) | copy-start | bytes 6148
  137.1 5.7 %copy-start.21 = (f32[1,512]{1,0:T(1,128)S(1)}, f32[1,512]{1,0:T(1,128)}, u32[]{:S(2)}) copy-start(f32[1,512]{1,0:T(1,128)} %get-tuple-element.45) | copy-start | bytes 6148
  137.1 5.7 %copy-start.22 = (f32[1,512]{1,0:T(1,128)S(1)}, f32[1,512]{1,0:T(1,128)}, u32[]{:S(2)}) copy-start(f32[1,512]{1,0:T(1,128)} %get-tuple-element.46) | copy-start | bytes 6148
  137.1 5.7 %copy-start.23 = (f32[1,512]{1,0:T(1,128)S(1)}, f32[1,512]{1,0:T(1,128)}, u32[]{:S(2)}) copy-start(f32[1,512]{1,0:T(1,128)} %get-tuple-element.47) | copy-start | bytes 6148
  137.1 5.7 %copy-start.24 = (f32[1,512]{1,0:T(1,128)S(1)}, f32[1,512]{1,0:T(1,128)}, u32[]{:S(2)}) copy-start(f32[1,512]{1,0:T(1,128)} %get-tuple-element.48) | copy-start | bytes 6148
  (9 other events, 15.8 us)
Sparse Core Ops, SparseCore 0:
  112.2 69.8 reduce-scatter.1

commit v2 on v1

--- a/solution.py
+++ b/solution.py
@@ -12,12 +12,6 @@
 norm_epsilon = 1e-05
 MESH = pl.DeviceIdType.MESH
 VMEM = pltpu.VMEM
-
-
-def passed_along(value, axis, steps):
-    count = lax.axis_size(axis)
-    leading, last = (max(0, -steps), min(count, count - steps))
-    return lax.ppermute(value, axis, [(source, source + steps) for source in range(leading, last)])
 
 
 def lanes(index, width):
@@ -253,6 +247,172 @@
         scratch_shapes=[dma((pieces,))] * 6 + [dma((1,))],
         compiler_params=pltpu.CompilerParams(collective_id=2, has_side_effects=True),
     )(mix)
+
+
+def tail_kernel(
+    group,
+    narrow,
+    reach,
+    parts_ref,
+    grad_ref,
+    hat_ref,
+    stat_ref,
+    taps_ref,
+    value_ref,
+    gate_ref,
+    proj_ref,
+    dvalue_ref,
+    dgate_ref,
+    stats,
+    next_stats,
+    next_grad,
+    next_hat,
+    extended,
+    pair_in,
+    pair_sum,
+    others,
+    *sems,
+):
+    t_s, t_r, v_s, v_r, h_s, h_r, x_s, x_r, z_s, z_r = sems
+    f32 = jnp.float32
+    me, t, near, far, cross = places(group, narrow)
+    rows, cols = grad_ref.shape
+    halo = next_grad.shape[0]
+    pairs = group // 2
+    parity = lax.rem(me, 2)
+    half = me // 2
+    partner = me + 1 - 2 * parity
+    ahead, behind = lax.rem(me + 1, group), lax.rem(me + group - 1, group)
+    siblings = [lax.rem(t + o, narrow) for o in range(1, narrow)]
+    alike = [lax.rem(half + o, pairs) for o in range(1, pairs)]
+    everyone = [t] + siblings
+    meet(
+        [(me, p) for p in siblings]
+        + [(ahead, p) for p in everyone]
+        + [(behind, p) for p in everyone]
+        + [(partner, t)]
+        + [(2 * q + parity, t) for q in alike]
+    )
+    sends = []
+    for k, p in enumerate(siblings):
+        sends.append(remote(stat_ref, stats.at[k], t_s.at[k], t_r.at[k], me, p))
+    for k, p in enumerate(everyone):
+        sends.append(remote(stat_ref, next_stats.at[k], v_s.at[k], v_r.at[k], behind, p))
+    sends.append(remote(grad_ref.at[pl.ds(0, halo)], next_grad, h_s.at[0], h_r.at[0], behind, t))
+    sends.append(remote(hat_ref.at[pl.ds(0, halo)], next_hat, h_s.at[1], h_r.at[1], behind, t))
+    for c in sends:
+        c.start()
+
+    def swap(q):
+        return remote(parts_ref.at[2 * q + 1 - parity], pair_in.at[q], x_s.at[q], x_r.at[q], partner, t)
+
+    def scatter(q):
+        return remote(pair_sum.at[q], others.at[half], z_s.at[q], z_r.at[half], 2 * q + parity, t)
+
+    order = alike + [half]
+    for q in order:
+        swap(q).start()
+    for c in sends:
+        c.wait_recv()
+
+    channels = cols * narrow
+
+    def finished(grad, hat, total, own):
+        total = jnp.transpose(total)
+        deviation = jnp.transpose(own)[:, 2:3]
+        count = grad.shape[0]
+        first, second = total[:count, 0:1] / channels, total[:count, 1:2] / channels
+        return deviation[:count] * (grad - first - hat * second)
+
+    total = stat_ref[...]
+    following = next_stats[0]
+    for k in range(narrow - 1):
+        total = total + stats[k]
+        following = following + next_stats[k + 1]
+    extended[pl.ds(0, rows), :] = finished(grad_ref[...], hat_ref[...], total, stat_ref[...])
+    beyond = finished(next_grad[...], next_hat[...], following, next_stats[0])
+    extended[pl.ds(rows, halo), :] = jnp.where(me == group - 1, jnp.zeros_like(beyond), beyond)
+
+    step = 32
+    strips = cols // 128
+
+    def convolve(index, carry):
+        start = pl.multiple_of((index // strips) * step, step)
+        column = lanes(lax.rem(index, strips), 128)
+        total = jnp.zeros((step, 128), f32)
+        window = extended[pl.ds(start, step + halo), column]
+        for turn in range(8):
+            shifted = window if turn == 0 else pltpu.roll(window, step + halo - turn, 0)
+            for j in range(turn, reach, 8):
+                total = total + taps_ref[reach - 1 - j : reach - j, column] * shifted[j - turn : j - turn + step]
+        place = (pl.ds(start, step), column)
+        sig = jax.nn.sigmoid(gate_ref[place].astype(f32))
+        dvalue_ref[place] = (total * sig).astype(dvalue_ref.dtype)
+        dgate_ref[place] = (total * value_ref[place].astype(f32) * sig * (1.0 - sig)).astype(dgate_ref.dtype)
+        return carry
+
+    turns = rows // step * strips
+    marks = [turns * i // pairs for i in range(pairs + 1)]
+    for i, q in enumerate(order):
+        lax.fori_loop(marks[i], marks[i + 1], convolve, 0)
+        swap(q).wait_recv()
+        both = parts_ref[2 * q + parity].astype(f32) + pair_in[q].astype(f32)
+        if i < pairs - 1:
+            pair_sum[q] = both.astype(pair_sum.dtype)
+            scatter(q).start()
+        else:
+            proj_ref[...] = both
+    for q in alike:
+        remote(pair_sum.at[q], others.at[q], z_s.at[q], z_r.at[q], 2 * q + parity, t).wait_recv()
+    proj = proj_ref[...]
+    for q in alike:
+        proj = proj + others[q].astype(f32)
+    proj_ref[...] = proj
+    for c in sends:
+        c.wait_send()
+    for q in order:
+        swap(q).wait_send()
+    for q in alike:
+        scatter(q).wait_send()
+
+
+def tail(parts, grad, hat, stat, taps, value_pre, gate_pre):
+    group, block, model = parts.shape
+    rows, cols = grad.shape
+    narrow = lax.axis_size("tp")
+    reach = taps.shape[0]
+    halo = -(-(reach - 1) // 8) * 8
+    pairs = group // 2
+    f32 = jnp.float32
+    dma = pltpu.SemaphoreType.DMA
+    return pl.pallas_call(
+        functools.partial(tail_kernel, group, narrow, reach),
+        out_shape=(
+            jax.ShapeDtypeStruct((block, model), f32),
+            jax.ShapeDtypeStruct((rows, cols), value_pre.dtype),
+            jax.ShapeDtypeStruct((rows, cols), gate_pre.dtype),
+        ),
+        in_specs=[pl.BlockSpec(memory_space=VMEM)] * 7,
+        out_specs=[pl.BlockSpec(memory_space=VMEM)] * 3,
+        scratch_shapes=[
+            VMEM((narrow - 1,) + stat.shape, f32),
+            VMEM((narrow,) + stat.shape, f32),
+            VMEM((halo, cols), f32),
+            VMEM((halo, cols), f32),
+            VMEM((rows + halo, cols), f32),
+            VMEM((pairs, block, model), parts.dtype),
+            VMEM((pairs, block, model), parts.dtype),
+            VMEM((pairs, block, model), parts.dtype),
+            dma((narrow - 1,)),
+            dma((narrow - 1,)),
+            dma((narrow,)),
+            dma((narrow,)),
+            dma((2,)),
+            dma((2,)),
+        ]
+        + [dma((pairs,))] * 4,
+        compiler_params=pltpu.CompilerParams(collective_id=3, has_side_effects=True),
+    )(parts, grad, hat, stat, taps, value_pre, gate_pre)
 
 
 def per_device(
@@ -339,14 +499,9 @@
     normalized_output = normalized_input * channel_norm_gain[None, :]
     sigma_conv = jax.nn.sigmoid(normalized_output)
     act_conv = (normalized_output * sigma_conv).astype(bf16)
-    grad_proj = lax.psum_scatter(
-        lax.dot_general(act_conv, mix_full, (((0,), (0,)), ((), ())), preferred_element_type=f32).astype(
-            bf16
-        ),
-        "sp",
-        scatter_dimension=0,
-        tiled=True,
-    ).astype(f32)
+    partial_proj = lax.dot_general(
+        act_conv, mix_full, (((0,), (0,)), ((), ())), preferred_element_type=f32
+    ).astype(bf16)
     d_act_conv = jnp.dot(mix_full, w_proj.T, preferred_element_type=f32)
     normalized_gradient = (
         d_act_conv
@@ -354,28 +509,23 @@
         * (1.0 + normalized_output * (1.0 - sigma_conv))
         * channel_norm_gain[None, :]
     )
-    first_term_gradient, second_term_gradient = lax.psum(
-        (
+    terms = jnp.stack(
+        [
             jnp.sum(normalized_gradient, axis=1),
             jnp.sum(normalized_gradient * normalized_input, axis=1),
-        ),
-        "tp",
-    )
-    convolution_gradient = inverse_deviation * (
-        normalized_gradient
-        - (first_term_gradient / channel_total)[:, None]
-        - normalized_input * (second_term_gradient / channel_total)[:, None]
-    )
-    reach = taps.shape[0]
-    following = passed_along(convolution_gradient[: reach - 1], "sp", -1)
-    extended = jnp.concatenate([convolution_gradient, following], axis=0)
-    d_glu = jnp.zeros_like(convolution_gradient)
-    for offset in range(reach):
-        begin = reach - 1 - offset
-        d_glu = d_glu + taps[offset][None, :] * extended[begin : begin + tok_rows]
-    gate_sig = jax.nn.sigmoid(gate_pre.astype(f32))
-    grad_value = (d_glu * gate_sig).astype(bf16)
-    grad_gate = (d_glu * value_pre.astype(f32) * gate_sig * (1.0 - gate_sig)).astype(bf16)
+            inverse_deviation[:, 0],
+        ]
+    )
+    terms = jnp.pad(terms, ((0, 8 - terms.shape[0]), (0, 0)))
+    grad_proj, grad_value, grad_gate = tail(
+        partial_proj.reshape(group_size, local_cols // group_size, model_width),
+        normalized_gradient,
+        normalized_input,
+        terms,
+        taps,
+        value_pre,
+        gate_pre,
+    )
     return (
         grad_gate_part[None],
         grad_up_part[None],

time: 191 us -> 172 us (0.901)
  Pallas kernels: 80.8 us -> 123 us
  waiting for transfers between devices: 25.9 us -> 0 us
  between operations: 14.5 us -> 0.84 us
  other arithmetic: 19.1 us -> 5.76 us
  blocking collectives: 7.03 us -> 0 us
    pallas_call x0 -> x1, Pallas kernels: none -> 41.9 us  [tail(): pl.pallas_call(functools.partial(tail_kernel, group, narrow, reach), out_...]
    reduce_scatter x1 -> x0, waiting for transfers between devices: 25.8 us -> none  [per_device(): lax.psum_scatter(lax.dot_general(act_conv, mix_full, (((0,), (0,)), ((),...]
    convert_element_type x3 -> x0, other arithmetic: 15.2 us -> none  [the longest x1 12.6 us: per_device(): (d_glu * value_pre.astype(f32) * gate_sig * (1.0 - gate_sig)).astype(bf16)]
    psum x1 -> x0, blocking collectives: 7.03 us -> none  [per_device(): lax.psum((jnp.sum(normalized_gradient, axis=1), jnp.sum(normalized_gradie...]
    slice x3 -> x0, local copies, waits for them, and re-layouts: 3.43 us -> none  [the longest x2 2.79 us: per_device(): d_glu = d_glu + taps[offset][None, :] * extended[begin:begin + tok_rows]]
    unnamed x64 -> x31, local copies, waits for them, and re-layouts: 8.38 us -> 9.78 us
  transfers between devices with their start and end apart: 2 -> 0, of which waited for: 1 -> 0; matrix products, arithmetic and copies ran while one was open for 18% -> 0% of each run, Pallas kernels for 0% -> 0%
where the time goes in v2:
time: 172 us; the launch traced here: 171 us
  Pallas kernels  123 us (72%)
  matrix products  30.2 us (18%)
  local copies, waits for them, and re-layouts  11.5 us (7%)
  other arithmetic  5.76 us (3%)
    pallas_call x1, Pallas kernels, tail(): pl.pallas_call(functools.partial(tail_kernel, group, narrow, reach), out_...  41.9 us
    pallas_call x1, Pallas kernels, dispatch(): pl.pallas_call(functools.partial(dispatch_kernel, group, narrow, width),...  35.4 us
    pallas_call x1, Pallas kernels, return_home(): pl.pallas_call(functools.partial(return_kernel, group, narrow, width), ou...  34.3 us
    pallas_call x1, Pallas kernels, widen(): pl.pallas_call(functools.partial(widen_kernel, narrow, width, pieces), ou...  11.1 us
    unnamed x31, local copies, waits for them, and re-layouts  9.78 us
    dot_general x1, matrix products, per_device(): d_act = jnp.dot(rows_cot, down_weight.T, preferred_element_type=f32)  4.2 us
    dot_general x1, matrix products, per_device(): d_act_conv = jnp.dot(mix_full, w_proj.T, preferred_element_type=f32)  3.78 us

profile of v2, /device:TPU:0, one launch (start us, length us, event | category | flops | bytes accessed | tf_op | source)
XLA Modules:
  0.0 171.0 jit_solution(3109892202918991427)
XLA Ops:
  0.6 0.9 fusion.65
  3.3 1.1 convert_reduce_fusion
  5.0 1.2 fusion.36
  6.2 3.1 %fusion.6 = f32[768,256]{1,0:T(8,128)} fusion(bf16[1,768,2048]{2,1,0:T(8,128)(2,1)S(1)} %copy-done, bf16[1,2048,256]{2,1,0:T(8,128)(2,1)} %param.17), kind=kOutput, calls=%fused_computation.7 | convolution fusion | flops 805306368 | bytes 4980736 | tf_op jit(solution)/shard_map/dot_general | solution.py:470
  9.3 1.9 %fusion.4 = f32[768,256]{1,0:T(8,128)} fusion(bf16[1,768,2048]{2,1,0:T(8,128)(2,1)S(1)} %copy-done, bf16[1,2048,256]{2,1,0:T(8,128)(2,1)S(1)} %copy-done.2), kind=kOutput, calls=%fused_computation.5 | convolution fusion | flops 805306368 | bytes 4980736 | tf_op jit(solution)/shard_map/dot_general | solution.py:471
  11.4 1.5 convolution_convert_fusion.2
  12.8 35.4 %shard_map.172 = (bf16[8,96,2048]{2,1,0:T(8,128)(2,1)}, f32[4,2,256]{2,1,0:T(2,128)}) custom-call(bf16[8,96,512]{2,1,0:T(8,128)(2,1)} %bitcast.73, f32[2,256]{1,0:T(2,128)} %pad_maximum_fusion.stat_ref), custom_call_target="tpu_custom_call" | custom-call | tf_op jit(solution)/shard_map/pallas_call | solution.py:106
  49.6 4.2 %select_convert_fusion = (bf16[768,256]{1,0:T(8,128)(2,1)S(1)}, bf16[768,256]{1,0:T(8,128)(2,1)S(1)}) fusion(f32[768,256]{1,0:T(8,128)} %fusion.4, f32[768,256]{1,0:T(8,128)} %fusion.6, bf16[768,2048]{1,0:T(8,128)(2,1)} %bitcast.93, bf16[1,256,2048]{2,1,0:T(8,128)(2,1)} %param.19), kind=kOutput, calls=%fused_computation.33 | convolution fusion | flops 809828352 | bytes 6553600 | tf_op jit(solution)/shard_map/dot_general | solution.py:477
  53.8 2.1 %fusion.14 = bf16[1,256,2048]{2,1,0:T(8,128)(2,1)} fusion(bf16[768,2048]{1,0:T(8,128)(2,1)S(1)} %bitcast.94, f32[768,256]{1,0:T(8,128)S(1)} %copy-done.11, f32[768,256]{1,0:T(8,128)S(1)} %copy-done.12), kind=kOutput, calls=%fused_computation.13 | convolution fusion | flops 807796736 | bytes 5767168 | tf_op jit(solution)/shard_map/dot_general | solution.py:476
  56.0 2.0 %fusion.15 = bf16[1,2048,256]{1,2,0:T(8,128)(2,1)} fusion(bf16[768,256]{1,0:T(8,128)(2,1)S(1)} %get-tuple-element.28, bf16[1,768,2048]{2,1,0:T(8,128)(2,1)S(1)} %copy-done), kind=kOutput, calls=%fused_computation.14 | convolution fusion | flops 805830656 | bytes 4587520 | tf_op jit(solution)/shard_map/dot_general | solution.py:485
  58.0 2.3 %copy.20 = bf16[1,2048,256]{2,1,0:T(8,128)(2,1)} copy(bf16[1,2048,256]{1,2,0:T(8,128)(2,1)} %fusion.15) | data formatting | bytes 2097152
  60.2 2.0 %fusion.18 = bf16[1,2048,256]{1,2,0:T(8,128)(2,1)} fusion(bf16[768,256]{1,0:T(8,128)(2,1)S(1)} %get-tuple-element.29, bf16[1,768,2048]{2,1,0:T(8,128)(2,1)S(1)} %copy-done), kind=kOutput, calls=%fused_computation.15 | convolution fusion | flops 805830656 | bytes 4587520 | tf_op jit(solution)/shard_map/dot_general | solution.py:484
  62.2 2.3 %copy.19 = bf16[1,2048,256]{2,1,0:T(8,128)(2,1)} copy(bf16[1,2048,256]{1,2,0:T(8,128)(2,1)} %fusion.18) | data formatting | bytes 2097152
  64.4 2.3 %fusion.28 = f32[768,2048]{1,0:T(8,128)S(1)} fusion(bf16[768,256]{1,0:T(8,128)(2,1)S(1)} %get-tuple-element.29, bf16[1,2048,256]{2,1,0:T(8,128)(2,1)} %param.17), kind=kOutput, calls=%fused_computation.26 | convolution fusion | flops 805306368 | bytes 7733248 | tf_op jit(solution)/shard_map/dot_general | solution.py:486
  66.8 2.7 %add_convert_fusion = bf16[768,2048]{1,0:T(8,128)(2,1)} fusion(f32[768,2048]{1,0:T(8,128)S(1)} %fusion.28, bf16[768,256]{1,0:T(8,128)(2,1)S(1)} %copy-done.5, bf16[1,2048,256]{2,1,0:T(8,128)(2,1)S(1)} %copy-done.3), kind=kOutput, calls=%fused_computation | convolution fusion | flops 808452096 | bytes 10878976 | tf_op jit(solution)/shard_map/dot_general | solution.py:487
  69.5 34.3 %shard_map.173 = bf16[8,96,512]{2,1,0:T(8,128)(2,1)} custom-call(bf16[8,96,2048]{2,1,0:T(8,128)(2,1)} %bitcast.71), custom_call_target="tpu_custom_call" | custom-call | tf_op jit(solution)/shard_map/pallas_call | solution.py:182
  103.8 2.3 %fusion.23.mix_ref = bf16[256,512]{1,0:T(8,128)(2,1)} fusion(bf16[768,512]{1,0:T(8,128)(2,1)} %bitcast.74, bf16[256,512]{1,0:T(8,128)(2,1)S(1)} %copy-done.6, s32[256]{0:T(256)S(1)} %bitcast.78, s32[256]{0:T(256)S(1)} %bitcast.76), kind=kOutput, calls=%fused_computation.21 | convolution fusion | flops 203292672 | bytes 1312768 | tf_op jit(solution)/shard_map/dot_general | solution.py:490
  106.0 11.1 %shard_map.174 = bf16[256,2048]{1,0:T(8,128)(2,1)} custom-call(bf16[256,512]{1,0:T(8,128)(2,1)} %fusion.23.mix_ref), custom_call_target="tpu_custom_call" | custom-call | tf_op jit(solution)/shard_map/pallas_call | solution.py:242
  117.2 3.8 %fusion.64 = (f32[256]{0:T(256)S(1)}, f32[256]{0:T(256)S(1)}, f32[256,512]{1,0:T(8,128)}, f32[256,512]{1,0:T(8,128)}) fusion(f32[256]{0:T(256)S(1)} %copy-done.8, f32[256]{0:T(256)S(1)} %bitcast.84, bf16[256,512]{1,0:T(8,128)(2,1)} %param.21, f32[512]{0:T(512)S(1)} %copy-done.10, bf16[256,2048]{1,0:T(8,128)(2,1)} %shard_map.174, bf16[512,2048]{1,0:T(8,128)(2,1)} %param.20), kind=kOutput, calls=%fused_computation.88 | convolution fusion | flops 538967552 | bytes 4462592 | tf_op jit(solution)/shard_map/dot_general | solution.py:505
  121.6 2.3 %convolution_convert_fusion = bf16[512,2048]{1,0:T(8,128)(2,1)} fusion(bf16[256,2048]{1,0:T(8,128)(2,1)S(1)} %copy-done.1, f32[512]{0:T(512)S(1)} %copy-done.10, bf16[256,512]{1,0:T(8,128)(2,1)S(1)} %copy-done.7, f32[256]{0:T(256)S(1)} %copy-done.8, f32[256]{0:T(256)S(1)} %bitcast.85), kind=kOutput, calls=%fused_computation.9 | convolution fusion | flops 539099136 | bytes 3411968 | tf_op jit(solution)/shard_map/dot_general | solution.py:502
  123.9 41.9 %shard_map.175 = (f32[64,2048]{1,0:T(8,128)}, bf16[256,512]{1,0:T(8,128)(2,1)}, bf16[256,512]{1,0:T(8,128)(2,1)}) custom-call(bf16[8,64,2048]{2,1,0:T(8,128)(2,1)} %bitcast.72, f32[256,512]{1,0:T(8,128)} %get-tuple-element.42.grad_ref, f32[256,512]{1,0:T(8,128)} %get-tuple-element.30.hat_ref, f32[8,256]{1,0:T(8,128)} %select_maximum_fusion.stat_ref, ...), custom_call_target="tpu_custom_call" | custom-call | tf_op jit(solution)/shard_map/pallas_call | solution.py:388
  165.8 1.9 %copy.24 = f32[64,2048]{1,0:T(8,128)} copy(f32[64,2048]{1,0:T(8,128)} %get-tuple-element.54) | data formatting | bytes 1048576
  167.7 1.7 copy.25
  169.3 1.7 copy.26
  (37 shorter events, 4.5 us)
Async XLA Ops:
  0.6 5.6 %copy-start = (bf16[1,768,2048]{2,1,0:T(8,128)(2,1)S(1)}, bf16[1,768,2048]{2,1,0:T(8,128)(2,1)}, u32[]{:S(2)}) copy-start(bf16[1,768,2048]{2,1,0:T(8,128)(2,1)} %param.16) | copy-start | bytes 9437188
  5.0 4.3 %copy-start.2 = (bf16[1,2048,256]{2,1,0:T(8,128)(2,1)S(1)}, bf16[1,2048,256]{2,1,0:T(8,128)(2,1)}, u32[]{:S(2)}) copy-start(bf16[1,2048,256]{2,1,0:T(8,128)(2,1)} %param.18) | copy-start | bytes 3145732
  49.6 4.2 %copy-start.9 = (bf16[8,96,2048]{2,1,0:T(8,128)(2,1)S(1)}, bf16[8,96,2048]{2,1,0:T(8,128)(2,1)}, u32[]{:S(2)}) copy-start(bf16[8,96,2048]{2,1,0:T(8,128)(2,1)} %get-tuple-element.11) | copy-start | bytes 9437188
  49.6 4.2 %copy-start.11 = (f32[768,256]{1,0:T(8,128)S(1)}, f32[768,256]{1,0:T(8,128)}, u32[]{:S(2)}) copy-start(f32[768,256]{1,0:T(8,128)} %fusion.6) | copy-start | bytes 2359300
  49.6 4.2 %copy-start.12 = (f32[768,256]{1,0:T(8,128)S(1)}, f32[768,256]{1,0:T(8,128)}, u32[]{:S(2)}) copy-start(f32[768,256]{1,0:T(8,128)} %fusion.4) | copy-start | bytes 2359300
  53.8 2.2 %copy-start.4 = (bf16[768,256]{1,0:T(8,128)(2,1)}, bf16[768,256]{1,0:T(8,128)(2,1)S(1)}, u32[]{:S(2)}) copy-start(bf16[768,256]{1,0:T(8,128)(2,1)S(1)} %get-tuple-element.28) | copy-start | bytes 1179652
  64.4 2.4 %copy-start.3 = (bf16[1,2048,256]{2,1,0:T(8,128)(2,1)S(1)}, bf16[1,2048,256]{2,1,0:T(8,128)(2,1)}, u32[]{:S(2)}) copy-start(bf16[1,2048,256]{2,1,0:T(8,128)(2,1)} %param.18) | copy-start | bytes 3145732
  64.4 2.4 %copy-start.5 = (bf16[768,256]{1,0:T(8,128)(2,1)S(1)}, bf16[768,256]{1,0:T(8,128)(2,1)}, u32[]{:S(2)}) copy-start(bf16[768,256]{1,0:T(8,128)(2,1)} %copy-done.4) | copy-start | bytes 1179652
  69.5 34.3 %copy-start.6 = (bf16[256,512]{1,0:T(8,128)(2,1)S(1)}, bf16[256,512]{1,0:T(8,128)(2,1)}, u32[]{:S(2)}) copy-start(bf16[256,512]{1,0:T(8,128)(2,1)} %param.13) | copy-start | bytes 786436
  69.5 47.7 %copy-start.8 = (f32[256]{0:T(256)S(1)}, f32[256]{0:T(256)}, u32[]{:S(2)}) copy-start(f32[256]{0:T(256)} %add_rsqrt_fusion.1) | copy-start | bytes 3076
  69.5 47.7 %copy-start.10 = (f32[512]{0:T(512)S(1)}, f32[512]{0:T(512)}, u32[]{:S(2)}) copy-start(f32[512]{0:T(512)} %param.22) | copy-start | bytes 6148
  117.2 4.4 %copy-start.1 = (bf16[256,2048]{1,0:T(8,128)(2,1)S(1)}, bf16[256,2048]{1,0:T(8,128)(2,1)}, u32[]{:S(2)}) copy-start(bf16[256,2048]{1,0:T(8,128)(2,1)} %shard_map.174) | copy-start | bytes 3145732
  117.2 4.4 %copy-start.7 = (bf16[256,512]{1,0:T(8,128)(2,1)S(1)}, bf16[256,512]{1,0:T(8,128)(2,1)}, u32[]{:S(2)}) copy-start(bf16[256,512]{1,0:T(8,128)(2,1)} %param.21) | copy-start | bytes 786436

commit v3 on v2

--- a/solution.py
+++ b/solution.py
@@ -25,6 +25,10 @@
     return me, t, near, far, lax.rem(near + narrow // 2, narrow)
 
 
+def spread(group):
+    return sorted(range(1, group), key=lambda o: abs(2 * o - group))
+
+
 def remote(src, dst, send, recv, sp, tp):
     return pltpu.make_async_remote_copy(
         src_ref=src, dst_ref=dst, send_sem=send, recv_sem=recv, device_id=(sp, tp), device_id_type=MESH
@@ -38,10 +42,24 @@
     pl.semaphore_wait(barrier, len(peers))
 
 
-def dispatch_kernel(group, narrow, width, out_ref, stat_ref, rows_ref, stats_ref, *sems):
+def dispatch_kernel(
+    group,
+    narrow,
+    width,
+    out_ref,
+    stat_ref,
+    in_ref,
+    gate_ref,
+    up_ref,
+    rows_ref,
+    stats_ref,
+    gate_lin_ref,
+    up_lin_ref,
+    *sems,
+):
     a_s, a_r, n_s, n_r, f_s, f_r, m_s, m_r, t_s, t_r, l_s = sems
     me, t, near, far, cross = places(group, narrow)
-    sp_peers = [lax.rem(me + o, group) for o in range(1, group)]
+    sp_peers = [lax.rem(me + o, group) for o in spread(group)]
     meet([(p, t) for p in sp_peers] + [(me, near), (me, far), (me, cross)])
 
     def spot(s, column):
@@ -62,7 +80,7 @@
     own = pltpu.make_async_copy(out_ref.at[me], spot(me, t), l_s.at[1])
     own.start()
     own.wait()
-    order = [me] + [lax.rem(me + group - o, group) for o in range(1, group)]
+    order = [me] + [lax.rem(me + group - o, group) for o in spread(group)]
 
     def to_far(s):
         return remote(spot(s, t), spot(s, t), f_s.at[s], f_r.at[s], me, far)
@@ -73,18 +91,31 @@
     def onward(s):
         return remote(spot(s, far), spot(s, far), m_s.at[s], m_r.at[s], me, near)
 
+    def relay(s):
+        to_far(s).wait_recv()
+        onward(s).start()
+
+    turns = 8
+    count = in_ref.shape[0] // turns
+
+    def multiply(piece):
+        span = pl.ds(piece * count, count)
+        rows = in_ref[span, :]
+        gate_lin_ref[span, :] = jnp.dot(rows, gate_ref[...], preferred_element_type=jnp.float32)
+        up_lin_ref[span, :] = jnp.dot(rows, up_ref[...], preferred_element_type=jnp.float32)
+
+    lag = min(2, group)
     for i, s in enumerate(order):
         if i > 0:
             remote(out_ref.at[s], spot(s, t), a_s.at[s], a_r.at[s], s, t).wait_recv()
         to_far(s).start()
         to_near(s).start()
-        if i > 0:
-            prev = order[i - 1]
-            remote(spot(prev, far), spot(prev, far), f_s.at[prev], f_r.at[prev], me, far).wait_recv()
-            onward(prev).start()
-    last = order[-1]
-    remote(spot(last, far), spot(last, far), f_s.at[last], f_r.at[last], me, far).wait_recv()
-    onward(last).start()
+        if i >= lag:
+            relay(order[i - lag])
+        for piece in range(turns * i // group, turns * (i + 1) // group):
+            multiply(piece)
+    for s in order[group - lag :]:
+        relay(s)
     for s in order:
         to_far(s).wait_send()
         to_near(s).wait_send()
@@ -99,7 +130,7 @@
         c.wait_recv()
 
 
-def dispatch(outgoing, stat):
+def dispatch(outgoing, stat, rows_in, gate_weight, up_weight):
     group, capacity, width = outgoing.shape
     narrow = lax.axis_size("tp")
     dma = pltpu.SemaphoreType.DMA
@@ -108,18 +139,20 @@
         out_shape=(
             jax.ShapeDtypeStruct((group, capacity, narrow * width), outgoing.dtype),
             jax.ShapeDtypeStruct((narrow,) + stat.shape, stat.dtype),
+            jax.ShapeDtypeStruct((rows_in.shape[0], gate_weight.shape[1]), jnp.float32),
+            jax.ShapeDtypeStruct((rows_in.shape[0], up_weight.shape[1]), jnp.float32),
         ),
-        in_specs=[pl.BlockSpec(memory_space=VMEM)] * 2,
-        out_specs=[pl.BlockSpec(memory_space=VMEM)] * 2,
+        in_specs=[pl.BlockSpec(memory_space=VMEM)] * 5,
+        out_specs=[pl.BlockSpec(memory_space=VMEM)] * 4,
         scratch_shapes=[dma((group,))] * 8 + [dma((3,))] * 2 + [dma((2,))],
         compiler_params=pltpu.CompilerParams(collective_id=0, has_side_effects=True),
-    )(outgoing, stat)
+    )(outgoing, stat, rows_in, gate_weight, up_weight)
 
 
 def return_kernel(group, narrow, width, part_ref, home_ref, pair_buf, far_out, far_in, done, *sems):
     n_s, n_r, f_s, f_r, a_s, a_r, l_s = sems
     me, t, near, far, cross = places(group, narrow)
-    sp_peers = [lax.rem(me + o, group) for o in range(1, group)]
+    sp_peers = [lax.rem(me + o, group) for o in spread(group)]
     meet([(p, t) for p in sp_peers] + [(me, near), (me, far)])
     order = sp_peers + [me]
 
@@ -139,6 +172,7 @@
 
     for s in order:
         to_near(s, 1).start()
+    for s in order:
         to_near(s, 0).start()
     own = pltpu.make_async_copy(done.at[me], home_ref.at[me], l_s.at[0])
 
@@ -153,16 +187,13 @@
         else:
             own.start()
 
-    lag = min(2, group - 1)
-    for i, s in enumerate(order):
+    for s in order:
         to_near(s, 1).wait_recv()
         pair = part_ref[s, :, lanes(far, width)].astype(jnp.float32) + pair_buf[s, 1].astype(jnp.float32)
         far_out[s] = pair.astype(far_out.dtype)
         to_far(s).start()
-        if i >= lag:
-            finish(order[i - lag], i - lag)
-    for i in range(group - lag, group):
-        finish(order[i], i)
+    for i, s in enumerate(order):
+        finish(s, i)
     own.wait()
     for s in order:
         to_near(s, 0).wait_send()
@@ -258,11 +289,9 @@
     hat_ref,
     stat_ref,
     taps_ref,
-    value_ref,
-    gate_ref,
     proj_ref,
-    dvalue_ref,
-    dgate_ref,
+    others,
+    glu_ref,
     stats,
     next_stats,
     next_grad,
@@ -270,7 +299,6 @@
     extended,
     pair_in,
     pair_sum,
-    others,
     *sems,
 ):
     t_s, t_r, v_s, v_r, h_s, h_r, x_s, x_r, z_s, z_r = sems
@@ -307,7 +335,10 @@
         return remote(parts_ref.at[2 * q + 1 - parity], pair_in.at[q], x_s.at[q], x_r.at[q], partner, t)
 
     def scatter(q):
-        return remote(pair_sum.at[q], others.at[half], z_s.at[q], z_r.at[half], 2 * q + parity, t)
+        return remote(pair_sum.at[q], others.at[slot_of(half, q)], z_s.at[q], z_r.at[half], 2 * q + parity, t)
+
+    def slot_of(source, target):
+        return lax.rem(target - source + pairs, pairs) - 1
 
     order = alike + [half]
     for q in order:
@@ -345,10 +376,7 @@
             shifted = window if turn == 0 else pltpu.roll(window, step + halo - turn, 0)
             for j in range(turn, reach, 8):
                 total = total + taps_ref[reach - 1 - j : reach - j, column] * shifted[j - turn : j - turn + step]
-        place = (pl.ds(start, step), column)
-        sig = jax.nn.sigmoid(gate_ref[place].astype(f32))
-        dvalue_ref[place] = (total * sig).astype(dvalue_ref.dtype)
-        dgate_ref[place] = (total * value_ref[place].astype(f32) * sig * (1.0 - sig)).astype(dgate_ref.dtype)
+        glu_ref[pl.ds(start, step), column] = total
         return carry
 
     turns = rows // step * strips
@@ -363,11 +391,7 @@
         else:
             proj_ref[...] = both
     for q in alike:
-        remote(pair_sum.at[q], others.at[q], z_s.at[q], z_r.at[q], 2 * q + parity, t).wait_recv()
-    proj = proj_ref[...]
-    for q in alike:
-        proj = proj + others[q].astype(f32)
-    proj_ref[...] = proj
+        remote(pair_sum.at[q], others.at[slot_of(q, half)], z_s.at[q], z_r.at[q], 2 * q + parity, t).wait_recv()
     for c in sends:
         c.wait_send()
     for q in order:
@@ -376,7 +400,7 @@
         scatter(q).wait_send()
 
 
-def tail(parts, grad, hat, stat, taps, value_pre, gate_pre):
+def tail(parts, grad, hat, stat, taps):
     group, block, model = parts.shape
     rows, cols = grad.shape
     narrow = lax.axis_size("tp")
@@ -389,10 +413,10 @@
         functools.partial(tail_kernel, group, narrow, reach),
         out_shape=(
             jax.ShapeDtypeStruct((block, model), f32),
-            jax.ShapeDtypeStruct((rows, cols), value_pre.dtype),
-            jax.ShapeDtypeStruct((rows, cols), gate_pre.dtype),
+            jax.ShapeDtypeStruct((pairs - 1, block, model), parts.dtype),
+            jax.ShapeDtypeStruct((rows, cols), f32),
         ),
-        in_specs=[pl.BlockSpec(memory_space=VMEM)] * 7,
+        in_specs=[pl.BlockSpec(memory_space=VMEM)] * 5,
         out_specs=[pl.BlockSpec(memory_space=VMEM)] * 3,
         scratch_shapes=[
             VMEM((narrow - 1,) + stat.shape, f32),
@@ -400,7 +424,6 @@
             VMEM((halo, cols), f32),
             VMEM((halo, cols), f32),
             VMEM((rows + halo, cols), f32),
-            VMEM((pairs, block, model), parts.dtype),
             VMEM((pairs, block, model), parts.dtype),
             VMEM((pairs, block, model), parts.dtype),
             dma((narrow - 1,)),
@@ -412,7 +435,7 @@
         ]
         + [dma((pairs,))] * 4,
         compiler_params=pltpu.CompilerParams(collective_id=3, has_side_effects=True),
-    )(parts, grad, hat, stat, taps, value_pre, gate_pre)
+    )(parts, grad, hat, stat, taps)
 
 
 def per_device(
@@ -461,14 +484,14 @@
     stat = jnp.stack(
         [jnp.sum(convolution_filter, axis=1), jnp.sum(convolution_filter * convolution_filter, axis=1)]
     )
-    arrived, stats = dispatch(outgoing.reshape(group_size, capacity, local_cols), stat)
-    rows_cot = arrived.reshape(slot_rows, model_width)
     rows_in = expert_inputs[0]
     gate_weight = w_gate[0]
     up_weight = w_up[0]
     down_weight = w_down[0]
-    gate_lin = jnp.dot(rows_in, gate_weight, preferred_element_type=f32)
-    up_lin = jnp.dot(rows_in, up_weight, preferred_element_type=f32)
+    arrived, stats, gate_lin, up_lin = dispatch(
+        outgoing.reshape(group_size, capacity, local_cols), stat, rows_in, gate_weight, up_weight
+    )
+    rows_cot = arrived.reshape(slot_rows, model_width)
     gate_c = jnp.minimum(gate_lin, clamp_limit)
     up_c = jnp.clip(up_lin, -clamp_limit, clamp_limit)
     sigma = jax.nn.sigmoid(swish_alpha * gate_c)
@@ -517,15 +540,17 @@
         ]
     )
     terms = jnp.pad(terms, ((0, 8 - terms.shape[0]), (0, 0)))
-    grad_proj, grad_value, grad_gate = tail(
+    own_proj, other_proj, d_glu = tail(
         partial_proj.reshape(group_size, local_cols // group_size, model_width),
         normalized_gradient,
         normalized_input,
         terms,
         taps,
-        value_pre,
-        gate_pre,
-    )
+    )
+    grad_proj = own_proj + jnp.sum(other_proj.astype(f32), axis=0)
+    gate_sig = jax.nn.sigmoid(gate_pre.astype(f32))
+    grad_value = (d_glu * gate_sig).astype(bf16)
+    grad_gate = (d_glu * value_pre.astype(f32) * gate_sig * (1.0 - gate_sig)).astype(bf16)
     return (
         grad_gate_part[None],
         grad_up_part[None],

time: 172 us -> 163 us (0.948)
  matrix products: 30.2 us -> 23.9 us
  local copies, waits for them, and re-layouts: 11.5 us -> 5.54 us
  other arithmetic: 5.76 us -> 9.92 us
    unnamed x31 -> x38, local copies, waits for them, and re-layouts: 9.78 us -> 3.93 us
    pallas_call x1, Pallas kernels: 35.4 us -> 41.2 us  [dispatch(): pl.pallas_call(functools.partial(dispatch_kernel, group, narrow, width),...]
    pallas_call x1, Pallas kernels: 34.3 us -> 29.1 us  [return_home(): pl.pallas_call(functools.partial(return_kernel, group, narrow, width), ou...]
    dot_general x2 -> x0, matrix products: 4.95 us -> none  [the longest x1 3.09 us: per_device(): gate_lin = jnp.dot(rows_in, gate_weight, preferred_element_type=f32)]
    dot_general x1, matrix products: 1.96 us -> 3.94 us  [per_device(): jnp.dot(rows_in.T, d_gate, preferred_element_type=f32).astype(bf16)]
    add x0 -> x1, other arithmetic: none -> 1.89 us  [per_device(): grad_proj = own_proj + jnp.sum(other_proj.astype(f32), axis=0)]
where the time goes in v3:
time: 163 us; the launch traced here: 162 us
  Pallas kernels  122 us (75%)
  matrix products  23.9 us (15%)
  other arithmetic  9.92 us (6%)
  local copies, waits for them, and re-layouts  5.54 us (3%)
    pallas_call x1, Pallas kernels, dispatch(): pl.pallas_call(functools.partial(dispatch_kernel, group, narrow, width),...  41.2 us
    pallas_call x1, Pallas kernels, tail(): pl.pallas_call(functools.partial(tail_kernel, group, narrow, reach), out_...  40.5 us
    pallas_call x1, Pallas kernels, return_home(): pl.pallas_call(functools.partial(return_kernel, group, narrow, width), ou...  29.1 us
    pallas_call x1, Pallas kernels, widen(): pl.pallas_call(functools.partial(widen_kernel, narrow, width, pieces), ou...  11.3 us
    dot_general x1, matrix products, per_device(): jnp.dot(rows_in.T, d_gate, preferred_element_type=f32).astype(bf16)  3.94 us
    unnamed x38, local copies, waits for them, and re-layouts  3.93 us
    dot_general x1, matrix products, per_device(): d_act = jnp.dot(rows_cot, down_weight.T, preferred_element_type=f32)  3.89 us

profile of v3, /device:TPU:0, one launch (start us, length us, event | category | flops | bytes accessed | tf_op | source)
XLA Modules:
  0.0 162.4 jit_solution(17252788254037671290)
XLA Ops:
  0.6 0.9 fusion.47
  1.5 0.8 fusion.48
  2.5 0.8 multiply_add_fusion.1
  3.2 1.1 convert_reduce_fusion.1
  5.0 1.1 fusion.13
  6.3 1.5 convolution_convert_fusion.4
  7.7 41.2 %shard_map.172 = (bf16[8,96,2048]{2,1,0:T(8,128)(2,1)}, f32[4,2,256]{2,1,0:T(2,128)}, f32[768,256]{1,0:T(8,128)}, f32[768,256]{1,0:T(8,128)}) custom-call(bf16[8,96,512]{2,1,0:T(8,128)(2,1)} %bitcast.60, f32[2,256]{1,0:T(2,128)} %pad_maximum_fusion.stat_ref, bf16[768,2048]{1,0:T(8,128)(2,1)} %bitcast.58, bf16[2048,256]{1,0:T(8,128)(2,1)} %bitcast.56, ...), custom_call_target="tpu_custom_call" | custom-call | tf_op jit(solution)/shard_map/pallas_call | solution.py:137
  50.3 3.9 %select_convert_fusion = (bf16[768,256]{1,0:T(8,128)(2,1)S(1)}, bf16[768,256]{1,0:T(8,128)(2,1)S(1)}) fusion(f32[768,256]{1,0:T(8,128)} %get-tuple-element.15, f32[768,256]{1,0:T(8,128)} %get-tuple-element.13, bf16[768,2048]{1,0:T(8,128)(2,1)} %bitcast.80, bf16[1,256,2048]{2,1,0:T(8,128)(2,1)S(1)} %copy-done.14), kind=kOutput, calls=%fused_computation.21 | convolution fusion | flops 809828352 | bytes 6553600 | tf_op jit(solution)/shard_map/dot_general | solution.py:500
  54.2 2.1 %fusion.2 = bf16[1,256,2048]{2,1,0:T(8,128)(2,1)} fusion(bf16[768,2048]{1,0:T(8,128)(2,1)S(1)} %bitcast.81, f32[768,256]{1,0:T(8,128)S(1)} %copy-done.15, f32[768,256]{1,0:T(8,128)S(1)} %copy-done.16), kind=kOutput, calls=%fused_computation.7 | convolution fusion | flops 807796736 | bytes 5767168 | tf_op jit(solution)/shard_map/dot_general | solution.py:499
  56.4 1.0 fusion.1
  57.4 1.3 copy.20
  58.7 3.9 %fusion = bf16[1,2048,256]{1,2,0:T(8,128)(2,1)} fusion(bf16[768,256]{1,0:T(8,128)(2,1)S(1)} %get-tuple-element.33, bf16[1,768,2048]{2,1,0:T(8,128)(2,1)} %param.16), kind=kOutput, calls=%fused_computation.5 | convolution fusion | flops 805830656 | bytes 4587520 | tf_op jit(solution)/shard_map/dot_general | solution.py:507
  62.6 2.3 %copy.19 = bf16[1,2048,256]{2,1,0:T(8,128)(2,1)} copy(bf16[1,2048,256]{1,2,0:T(8,128)(2,1)} %fusion) | data formatting | bytes 2097152
  64.9 1.0 fusion.36
  66.2 2.7 %add_convert_fusion = bf16[768,2048]{1,0:T(8,128)(2,1)} fusion(f32[768,2048]{1,0:T(8,128)S(1)} %fusion.36, bf16[768,256]{1,0:T(8,128)(2,1)S(1)} %copy-done.7, bf16[1,2048,256]{2,1,0:T(8,128)(2,1)S(1)} %copy-done.2), kind=kOutput, calls=%fused_computation | convolution fusion | flops 808452096 | bytes 10878976 | tf_op jit(solution)/shard_map/dot_general | solution.py:510
  68.9 29.1 %shard_map.173 = bf16[8,96,512]{2,1,0:T(8,128)(2,1)} custom-call(bf16[8,96,2048]{2,1,0:T(8,128)(2,1)} %bitcast.55), custom_call_target="tpu_custom_call" | custom-call | tf_op jit(solution)/shard_map/pallas_call | solution.py:213
  98.0 2.3 %fusion.5.mix_ref = bf16[256,512]{1,0:T(8,128)(2,1)} fusion(bf16[768,512]{1,0:T(8,128)(2,1)} %bitcast.61, bf16[256,512]{1,0:T(8,128)(2,1)S(1)} %copy-done.8, s32[256]{0:T(256)S(1)} %bitcast.65, s32[256]{0:T(256)S(1)} %bitcast.63), kind=kOutput, calls=%fused_computation.14 | convolution fusion | flops 203292672 | bytes 1312768 | tf_op jit(solution)/shard_map/dot_general | solution.py:513
  100.3 11.3 %shard_map.174 = bf16[256,2048]{1,0:T(8,128)(2,1)} custom-call(bf16[256,512]{1,0:T(8,128)(2,1)} %fusion.5.mix_ref), custom_call_target="tpu_custom_call" | custom-call | tf_op jit(solution)/shard_map/pallas_call | solution.py:273
  111.6 3.1 %fusion.46 = (f32[256]{0:T(256)S(1)}, f32[256]{0:T(256)S(1)}, f32[256,512]{1,0:T(8,128)}, f32[256,512]{1,0:T(8,128)}) fusion(f32[256]{0:T(256)S(1)} %copy-done.12, f32[256]{0:T(256)S(1)} %bitcast.71, bf16[256,512]{1,0:T(8,128)(2,1)S(1)} %copy-done.9, f32[512]{0:T(512)S(1)} %copy-done.17, bf16[256,2048]{1,0:T(8,128)(2,1)} %shard_map.174, ...), kind=kOutput, calls=%fused_computation.84 | convolution fusion | flops 538967552 | bytes 4462592 | tf_op jit(solution)/shard_map/dot_general | solution.py:528
  115.3 2.3 %convolution_convert_fusion = bf16[512,2048]{1,0:T(8,128)(2,1)} fusion(bf16[256,2048]{1,0:T(8,128)(2,1)S(1)} %copy-done.4, f32[512]{0:T(512)S(1)} %copy-done.17, bf16[256,512]{1,0:T(8,128)(2,1)S(1)} %copy-done.9, f32[256]{0:T(256)S(1)} %copy-done.12, f32[256]{0:T(256)S(1)} %bitcast.72), kind=kOutput, calls=%fused_computation.1 | convolution fusion | flops 539099136 | bytes 3411968 | tf_op jit(solution)/shard_map/dot_general | solution.py:525
  117.6 40.5 %shard_map.175 = (f32[64,2048]{1,0:T(8,128)}, bf16[3,64,2048]{2,1,0:T(8,128)(2,1)}, f32[256,512]{1,0:T(8,128)}) custom-call(bf16[8,64,2048]{2,1,0:T(8,128)(2,1)} %bitcast.59, f32[256,512]{1,0:T(8,128)} %get-tuple-element.48.grad_ref, f32[256,512]{1,0:T(8,128)} %get-tuple-element.36.hat_ref, f32[8,256]{1,0:T(8,128)} %select_maximum_fusion.stat_ref, ...), custom_call_target="tpu_custom_call" | custom-call | tf_op jit(solution)/shard_map/pallas_call | solution.py:412
  158.2 1.4 convert_reduce_fusion
  159.5 1.9 %add.71 = f32[64,2048]{1,0:T(8,128)} add(f32[64,2048]{1,0:T(8,128)} %get-tuple-element.17, f32[64,2048]{1,0:T(8,128)S(1)} %convert_reduce_fusion) | non-fusion elementwise | flops 131072 | bytes 1572864 | tf_op jit(solution)/shard_map/add | solution.py:550
  161.4 1.0 multiply_convert_fusion.1
  (45 shorter events, 3.3 us)
Async XLA Ops:
  0.6 110.9 %copy-start = (bf16[512,2048]{1,0:T(8,128)(2,1)S(1)}, bf16[512,2048]{1,0:T(8,128)(2,1)}, u32[]{:S(2)}) copy-start(bf16[512,2048]{1,0:T(8,128)(2,1)} %param.20) | copy-start | bytes 6291460
  7.7 42.5 %copy-start.14 = (bf16[1,256,2048]{2,1,0:T(8,128)(2,1)S(1)}, bf16[1,256,2048]{2,1,0:T(8,128)(2,1)}, u32[]{:S(2)}) copy-start(bf16[1,256,2048]{2,1,0:T(8,128)(2,1)} %param.19) | copy-start | bytes 3145732
  50.3 3.9 %copy-start.13 = (bf16[8,96,2048]{2,1,0:T(8,128)(2,1)S(1)}, bf16[8,96,2048]{2,1,0:T(8,128)(2,1)}, u32[]{:S(2)}) copy-start(bf16[8,96,2048]{2,1,0:T(8,128)(2,1)} %get-tuple-element.14) | copy-start | bytes 9437188
  50.3 3.9 %copy-start.15 = (f32[768,256]{1,0:T(8,128)S(1)}, f32[768,256]{1,0:T(8,128)}, u32[]{:S(2)}) copy-start(f32[768,256]{1,0:T(8,128)} %get-tuple-element.13) | copy-start | bytes 2359300
  50.3 3.9 %copy-start.16 = (f32[768,256]{1,0:T(8,128)S(1)}, f32[768,256]{1,0:T(8,128)}, u32[]{:S(2)}) copy-start(f32[768,256]{1,0:T(8,128)} %get-tuple-element.15) | copy-start | bytes 2359300
  54.2 2.2 %copy-start.6 = (bf16[768,256]{1,0:T(8,128)(2,1)}, bf16[768,256]{1,0:T(8,128)(2,1)S(1)}, u32[]{:S(2)}) copy-start(bf16[768,256]{1,0:T(8,128)(2,1)S(1)} %get-tuple-element.32) | copy-start | bytes 1179652
  54.2 2.2 %copy-start.3 = (bf16[1,768,2048]{2,1,0:T(8,128)(2,1)S(1)}, bf16[1,768,2048]{2,1,0:T(8,128)(2,1)}, u32[]{:S(2)}) copy-start(bf16[1,768,2048]{2,1,0:T(8,128)(2,1)} %param.16) | copy-start | bytes 9437188
  58.7 6.2 %copy-start.1 = (bf16[1,2048,256]{2,1,0:T(8,128)(2,1)S(1)}, bf16[1,2048,256]{2,1,0:T(8,128)(2,1)}, u32[]{:S(2)}) copy-start(bf16[1,2048,256]{2,1,0:T(8,128)(2,1)} %param.17) | copy-start | bytes 3145732
  64.9 1.2 copy-start.2
  64.9 1.3 copy-start.7
  68.8 29.2 %copy-start.8 = (bf16[256,512]{1,0:T(8,128)(2,1)S(1)}, bf16[256,512]{1,0:T(8,128)(2,1)}, u32[]{:S(2)}) copy-start(bf16[256,512]{1,0:T(8,128)(2,1)} %param.13) | copy-start | bytes 786436
  68.8 42.7 %copy-start.9 = (bf16[256,512]{1,0:T(8,128)(2,1)S(1)}, bf16[256,512]{1,0:T(8,128)(2,1)}, u32[]{:S(2)}) copy-start(bf16[256,512]{1,0:T(8,128)(2,1)} %param.21) | copy-start | bytes 786436
  68.8 42.7 %copy-start.12 = (f32[256]{0:T(256)S(1)}, f32[256]{0:T(256)}, u32[]{:S(2)}) copy-start(f32[256]{0:T(256)} %add_rsqrt_fusion.1) | copy-start | bytes 3076
  68.9 42.7 %copy-start.17 = (f32[512]{0:T(512)S(1)}, f32[512]{0:T(512)}, u32[]{:S(2)}) copy-start(f32[512]{0:T(512)} %param.22) | copy-start | bytes 6148
  111.6 3.7 %copy-start.4 = (bf16[256,2048]{1,0:T(8,128)(2,1)S(1)}, bf16[256,2048]{1,0:T(8,128)(2,1)}, u32[]{:S(2)}) copy-start(bf16[256,2048]{1,0:T(8,128)(2,1)} %shard_map.174) | copy-start | bytes 3145732
  117.6 43.8 %copy-start.10 = (bf16[256,512]{1,0:T(8,128)(2,1)S(1)}, bf16[256,512]{1,0:T(8,128)(2,1)}, u32[]{:S(2)}) copy-start(bf16[256,512]{1,0:T(8,128)(2,1)} %param.24) | copy-start | bytes 786436
  117.6 43.8 %copy-start.11 = (bf16[256,512]{1,0:T(8,128)(2,1)S(1)}, bf16[256,512]{1,0:T(8,128)(2,1)}, u32[]{:S(2)}) copy-start(bf16[256,512]{1,0:T(8,128)(2,1)} %param.25) | copy-start | bytes 786436
  158.1 3.3 %copy-start.5 = (f32[256,512]{1,0:T(8,128)S(1)}, f32[256,512]{1,0:T(8,128)}, u32[]{:S(2)}) copy-start(f32[256,512]{1,0:T(8,128)} %get-tuple-element.19) | copy-start | bytes 1572868

commit v4 on v3

--- a/solution.py
+++ b/solution.py
@@ -25,8 +25,19 @@
     return me, t, near, far, lax.rem(near + narrow // 2, narrow)
 
 
-def spread(group):
-    return sorted(range(1, group), key=lambda o: abs(2 * o - group))
+def spread(pairs):
+    return sorted(range(1, pairs), key=lambda o: abs(2 * o - pairs))
+
+
+def around(me, group, sign):
+    pairs = group // 2
+    half, parity = me // 2, lax.rem(me, 2)
+    across = [
+        2 * lax.rem(half + pairs + sign * o, pairs) + (parity if side == 0 else 1 - parity)
+        for o in spread(pairs)
+        for side in range(2)
+    ]
+    return 2 * half + 1 - parity, across
 
 
 def remote(src, dst, send, recv, sp, tp):
@@ -59,7 +70,8 @@
 ):
     a_s, a_r, n_s, n_r, f_s, f_r, m_s, m_r, t_s, t_r, l_s = sems
     me, t, near, far, cross = places(group, narrow)
-    sp_peers = [lax.rem(me + o, group) for o in spread(group)]
+    partner, across = around(me, group, 1)
+    sp_peers = [partner] + across
     meet([(p, t) for p in sp_peers] + [(me, near), (me, far), (me, cross)])
 
     def spot(s, column):
@@ -80,7 +92,7 @@
     own = pltpu.make_async_copy(out_ref.at[me], spot(me, t), l_s.at[1])
     own.start()
     own.wait()
-    order = [me] + [lax.rem(me + group - o, group) for o in spread(group)]
+    order = [me, partner] + around(me, group, -1)[1]
 
     def to_far(s):
         return remote(spot(s, t), spot(s, t), f_s.at[s], f_r.at[s], me, far)
@@ -152,7 +164,8 @@
 def return_kernel(group, narrow, width, part_ref, home_ref, pair_buf, far_out, far_in, done, *sems):
     n_s, n_r, f_s, f_r, a_s, a_r, l_s = sems
     me, t, near, far, cross = places(group, narrow)
-    sp_peers = [lax.rem(me + o, group) for o in spread(group)]
+    partner, across = around(me, group, 1)
+    sp_peers = across + [partner]
     meet([(p, t) for p in sp_peers] + [(me, near), (me, far)])
     order = sp_peers + [me]
 
@@ -312,7 +325,9 @@
     partner = me + 1 - 2 * parity
     ahead, behind = lax.rem(me + 1, group), lax.rem(me + group - 1, group)
     siblings = [lax.rem(t + o, narrow) for o in range(1, narrow)]
-    alike = [lax.rem(half + o, pairs) for o in range(1, pairs)]
+    alike = [lax.rem(half + o, pairs) for o in spread(pairs)]
+    cut = parts_ref.shape[2] // 2
+    sides = [pl.ds(h * cut, cut) for h in range(2)]
     everyone = [t] + siblings
     meet(
         [(me, p) for p in siblings]
@@ -331,18 +346,32 @@
     for c in sends:
         c.start()
 
-    def swap(q):
-        return remote(parts_ref.at[2 * q + 1 - parity], pair_in.at[q], x_s.at[q], x_r.at[q], partner, t)
-
-    def scatter(q):
-        return remote(pair_sum.at[q], others.at[slot_of(half, q)], z_s.at[q], z_r.at[half], 2 * q + parity, t)
+    def swap(q, h):
+        side = sides[h]
+        return remote(
+            parts_ref.at[2 * q + 1 - parity, :, side],
+            pair_in.at[q, :, side],
+            x_s.at[q, h],
+            x_r.at[q, h],
+            partner,
+            t,
+        )
+
+    def passing(source, target, h):
+        slot = others.at[slot_of(source, target), :, sides[h]]
+        return slot, z_r.at[source, h]
+
+    def scatter(q, h):
+        slot, arrival = passing(half, q, h)
+        return remote(pair_sum.at[q, :, sides[h]], slot, z_s.at[q, h], arrival, 2 * q + parity, t)
 
     def slot_of(source, target):
         return lax.rem(target - source + pairs, pairs) - 1
 
     order = alike + [half]
     for q in order:
-        swap(q).start()
+        for h in range(2):
+            swap(q, h).start()
     for c in sends:
         c.wait_recv()
 
@@ -380,24 +409,28 @@
         return carry
 
     turns = rows // step * strips
-    marks = [turns * i // pairs for i in range(pairs + 1)]
+    marks = [turns * i // (2 * pairs) for i in range(2 * pairs + 1)]
     for i, q in enumerate(order):
-        lax.fori_loop(marks[i], marks[i + 1], convolve, 0)
-        swap(q).wait_recv()
-        both = parts_ref[2 * q + parity].astype(f32) + pair_in[q].astype(f32)
-        if i < pairs - 1:
-            pair_sum[q] = both.astype(pair_sum.dtype)
-            scatter(q).start()
-        else:
-            proj_ref[...] = both
+        for h in range(2):
+            lax.fori_loop(marks[2 * i + h], marks[2 * i + h + 1], convolve, 0)
+            swap(q, h).wait_recv()
+            both = parts_ref[2 * q + parity, :, sides[h]].astype(f32) + pair_in[q, :, sides[h]].astype(f32)
+            if i < pairs - 1:
+                pair_sum[q, :, sides[h]] = both.astype(pair_sum.dtype)
+                scatter(q, h).start()
+            else:
+                proj_ref[:, sides[h]] = both
     for q in alike:
-        remote(pair_sum.at[q], others.at[slot_of(q, half)], z_s.at[q], z_r.at[q], 2 * q + parity, t).wait_recv()
+        for h in range(2):
+            slot, arrival = passing(q, half, h)
+            remote(pair_sum.at[q, :, sides[h]], slot, z_s.at[q, h], arrival, 2 * q + parity, t).wait_recv()
     for c in sends:
         c.wait_send()
-    for q in order:
-        swap(q).wait_send()
-    for q in alike:
-        scatter(q).wait_send()
+    for h in range(2):
+        for q in order:
+            swap(q, h).wait_send()
+        for q in alike:
+            scatter(q, h).wait_send()
 
 
 def tail(parts, grad, hat, stat, taps):
@@ -433,7 +466,7 @@
             dma((2,)),
             dma((2,)),
         ]
-        + [dma((pairs,))] * 4,
+        + [dma((pairs, 2))] * 4,
         compiler_params=pltpu.CompilerParams(collective_id=3, has_side_effects=True),
     )(parts, grad, hat, stat, taps)
 

time: 163 us -> 160 us (0.982)
  Pallas kernels: 122 us -> 119 us
    pallas_call x1, Pallas kernels: 41.2 us -> 39.1 us  [dispatch(): pl.pallas_call(functools.partial(dispatch_kernel, group, narrow, width),...]
    pallas_call x1, Pallas kernels: 40.5 us -> 38.6 us  [tail(): pl.pallas_call(functools.partial(tail_kernel, group, narrow, reach), out_...]
where the time goes in v4:
time: 160 us; the launch traced here: 159 us
  Pallas kernels  119 us (74%)
  matrix products  23.9 us (15%)
  other arithmetic  9.92 us (6%)
  local copies, waits for them, and re-layouts  5.54 us (3%)
    pallas_call x1, Pallas kernels, dispatch(): pl.pallas_call(functools.partial(dispatch_kernel, group, narrow, width),...  39.1 us
    pallas_call x1, Pallas kernels, tail(): pl.pallas_call(functools.partial(tail_kernel, group, narrow, reach), out_...  38.6 us
    pallas_call x1, Pallas kernels, return_home(): pl.pallas_call(functools.partial(return_kernel, group, narrow, width), ou...  30 us
    pallas_call x1, Pallas kernels, widen(): pl.pallas_call(functools.partial(widen_kernel, narrow, width, pieces), ou...  11.3 us
    dot_general x1, matrix products, per_device(): jnp.dot(rows_in.T, d_gate, preferred_element_type=f32).astype(bf16)  3.94 us
    unnamed x38, local copies, waits for them, and re-layouts  3.93 us
    dot_general x1, matrix products, per_device(): d_act = jnp.dot(rows_cot, down_weight.T, preferred_element_type=f32)  3.89 us

profile of v4, /device:TPU:0, one launch (start us, length us, event | category | flops | bytes accessed | tf_op | source)
XLA Modules:
  0.0 159.3 jit_solution(995018439855645709)
XLA Ops:
  0.6 0.9 fusion.47
  1.5 0.8 fusion.48
  2.5 0.8 multiply_add_fusion.1
  3.2 1.1 convert_reduce_fusion.1
  5.0 1.1 fusion.13
  6.3 1.5 convolution_convert_fusion.4
  7.7 39.1 %shard_map.172 = (bf16[8,96,2048]{2,1,0:T(8,128)(2,1)}, f32[4,2,256]{2,1,0:T(2,128)}, f32[768,256]{1,0:T(8,128)}, f32[768,256]{1,0:T(8,128)}) custom-call(bf16[8,96,512]{2,1,0:T(8,128)(2,1)} %bitcast.60, f32[2,256]{1,0:T(2,128)} %pad_maximum_fusion.stat_ref, bf16[768,2048]{1,0:T(8,128)(2,1)} %bitcast.58, bf16[2048,256]{1,0:T(8,128)(2,1)} %bitcast.56, ...), custom_call_target="tpu_custom_call" | custom-call | tf_op jit(solution)/shard_map/pallas_call | solution.py:149
  48.2 3.9 %select_convert_fusion = (bf16[768,256]{1,0:T(8,128)(2,1)S(1)}, bf16[768,256]{1,0:T(8,128)(2,1)S(1)}) fusion(f32[768,256]{1,0:T(8,128)} %get-tuple-element.15, f32[768,256]{1,0:T(8,128)} %get-tuple-element.13, bf16[768,2048]{1,0:T(8,128)(2,1)} %bitcast.80, bf16[1,256,2048]{2,1,0:T(8,128)(2,1)S(1)} %copy-done.14), kind=kOutput, calls=%fused_computation.21 | convolution fusion | flops 809828352 | bytes 6553600 | tf_op jit(solution)/shard_map/dot_general | solution.py:533
  52.1 2.1 %fusion.2 = bf16[1,256,2048]{2,1,0:T(8,128)(2,1)} fusion(bf16[768,2048]{1,0:T(8,128)(2,1)S(1)} %bitcast.81, f32[768,256]{1,0:T(8,128)S(1)} %copy-done.15, f32[768,256]{1,0:T(8,128)S(1)} %copy-done.16), kind=kOutput, calls=%fused_computation.7 | convolution fusion | flops 807796736 | bytes 5767168 | tf_op jit(solution)/shard_map/dot_general | solution.py:532
  54.2 1.0 fusion.1
  55.3 1.3 copy.20
  56.6 3.9 %fusion = bf16[1,2048,256]{1,2,0:T(8,128)(2,1)} fusion(bf16[768,256]{1,0:T(8,128)(2,1)S(1)} %get-tuple-element.33, bf16[1,768,2048]{2,1,0:T(8,128)(2,1)} %param.16), kind=kOutput, calls=%fused_computation.5 | convolution fusion | flops 805830656 | bytes 4587520 | tf_op jit(solution)/shard_map/dot_general | solution.py:540
  60.5 2.3 %copy.19 = bf16[1,2048,256]{2,1,0:T(8,128)(2,1)} copy(bf16[1,2048,256]{1,2,0:T(8,128)(2,1)} %fusion) | data formatting | bytes 2097152
  62.8 1.0 fusion.36
  64.1 2.7 %add_convert_fusion = bf16[768,2048]{1,0:T(8,128)(2,1)} fusion(f32[768,2048]{1,0:T(8,128)S(1)} %fusion.36, bf16[768,256]{1,0:T(8,128)(2,1)S(1)} %copy-done.7, bf16[1,2048,256]{2,1,0:T(8,128)(2,1)S(1)} %copy-done.2), kind=kOutput, calls=%fused_computation | convolution fusion | flops 808452096 | bytes 10878976 | tf_op jit(solution)/shard_map/dot_general | solution.py:543
  66.8 30.0 %shard_map.173 = bf16[8,96,512]{2,1,0:T(8,128)(2,1)} custom-call(bf16[8,96,2048]{2,1,0:T(8,128)(2,1)} %bitcast.55), custom_call_target="tpu_custom_call" | custom-call | tf_op jit(solution)/shard_map/pallas_call | solution.py:226
  96.8 2.3 %fusion.5.mix_ref = bf16[256,512]{1,0:T(8,128)(2,1)} fusion(bf16[768,512]{1,0:T(8,128)(2,1)} %bitcast.61, bf16[256,512]{1,0:T(8,128)(2,1)S(1)} %copy-done.8, s32[256]{0:T(256)S(1)} %bitcast.65, s32[256]{0:T(256)S(1)} %bitcast.63), kind=kOutput, calls=%fused_computation.14 | convolution fusion | flops 203292672 | bytes 1312768 | tf_op jit(solution)/shard_map/dot_general | solution.py:546
  99.0 11.3 %shard_map.174 = bf16[256,2048]{1,0:T(8,128)(2,1)} custom-call(bf16[256,512]{1,0:T(8,128)(2,1)} %fusion.5.mix_ref), custom_call_target="tpu_custom_call" | custom-call | tf_op jit(solution)/shard_map/pallas_call | solution.py:286
  110.4 3.1 %fusion.46 = (f32[256]{0:T(256)S(1)}, f32[256]{0:T(256)S(1)}, f32[256,512]{1,0:T(8,128)}, f32[256,512]{1,0:T(8,128)}) fusion(f32[256]{0:T(256)S(1)} %copy-done.12, f32[256]{0:T(256)S(1)} %bitcast.71, bf16[256,512]{1,0:T(8,128)(2,1)S(1)} %copy-done.9, f32[512]{0:T(512)S(1)} %copy-done.17, bf16[256,2048]{1,0:T(8,128)(2,1)} %shard_map.174, ...), kind=kOutput, calls=%fused_computation.84 | convolution fusion | flops 538967552 | bytes 4462592 | tf_op jit(solution)/shard_map/dot_general | solution.py:561
  114.1 2.3 %convolution_convert_fusion = bf16[512,2048]{1,0:T(8,128)(2,1)} fusion(bf16[256,2048]{1,0:T(8,128)(2,1)S(1)} %copy-done.4, f32[512]{0:T(512)S(1)} %copy-done.17, bf16[256,512]{1,0:T(8,128)(2,1)S(1)} %copy-done.9, f32[256]{0:T(256)S(1)} %copy-done.12, f32[256]{0:T(256)S(1)} %bitcast.72), kind=kOutput, calls=%fused_computation.1 | convolution fusion | flops 539099136 | bytes 3411968 | tf_op jit(solution)/shard_map/dot_general | solution.py:558
  116.4 38.6 %shard_map.175 = (f32[64,2048]{1,0:T(8,128)}, bf16[3,64,2048]{2,1,0:T(8,128)(2,1)}, f32[256,512]{1,0:T(8,128)}) custom-call(bf16[8,64,2048]{2,1,0:T(8,128)(2,1)} %bitcast.59, f32[256,512]{1,0:T(8,128)} %get-tuple-element.48.grad_ref, f32[256,512]{1,0:T(8,128)} %get-tuple-element.36.hat_ref, f32[8,256]{1,0:T(8,128)} %select_maximum_fusion.stat_ref, ...), custom_call_target="tpu_custom_call" | custom-call | tf_op jit(solution)/shard_map/pallas_call | solution.py:445
  155.0 1.4 convert_reduce_fusion
  156.3 1.9 %add.71 = f32[64,2048]{1,0:T(8,128)} add(f32[64,2048]{1,0:T(8,128)} %get-tuple-element.17, f32[64,2048]{1,0:T(8,128)S(1)} %convert_reduce_fusion) | non-fusion elementwise | flops 131072 | bytes 1572864 | tf_op jit(solution)/shard_map/add | solution.py:583
  158.2 1.0 multiply_convert_fusion.1
  (45 shorter events, 3.3 us)
Async XLA Ops:
  0.6 109.7 %copy-start = (bf16[512,2048]{1,0:T(8,128)(2,1)S(1)}, bf16[512,2048]{1,0:T(8,128)(2,1)}, u32[]{:S(2)}) copy-start(bf16[512,2048]{1,0:T(8,128)(2,1)} %param.20) | copy-start | bytes 6291460
  7.7 40.4 %copy-start.14 = (bf16[1,256,2048]{2,1,0:T(8,128)(2,1)S(1)}, bf16[1,256,2048]{2,1,0:T(8,128)(2,1)}, u32[]{:S(2)}) copy-start(bf16[1,256,2048]{2,1,0:T(8,128)(2,1)} %param.19) | copy-start | bytes 3145732
  48.2 3.9 %copy-start.13 = (bf16[8,96,2048]{2,1,0:T(8,128)(2,1)S(1)}, bf16[8,96,2048]{2,1,0:T(8,128)(2,1)}, u32[]{:S(2)}) copy-start(bf16[8,96,2048]{2,1,0:T(8,128)(2,1)} %get-tuple-element.14) | copy-start | bytes 9437188
  48.2 3.9 %copy-start.15 = (f32[768,256]{1,0:T(8,128)S(1)}, f32[768,256]{1,0:T(8,128)}, u32[]{:S(2)}) copy-start(f32[768,256]{1,0:T(8,128)} %get-tuple-element.13) | copy-start | bytes 2359300
  48.2 3.9 %copy-start.16 = (f32[768,256]{1,0:T(8,128)S(1)}, f32[768,256]{1,0:T(8,128)}, u32[]{:S(2)}) copy-start(f32[768,256]{1,0:T(8,128)} %get-tuple-element.15) | copy-start | bytes 2359300
  52.1 2.2 %copy-start.6 = (bf16[768,256]{1,0:T(8,128)(2,1)}, bf16[768,256]{1,0:T(8,128)(2,1)S(1)}, u32[]{:S(2)}) copy-start(bf16[768,256]{1,0:T(8,128)(2,1)S(1)} %get-tuple-element.32) | copy-start | bytes 1179652
  52.1 2.2 %copy-start.3 = (bf16[1,768,2048]{2,1,0:T(8,128)(2,1)S(1)}, bf16[1,768,2048]{2,1,0:T(8,128)(2,1)}, u32[]{:S(2)}) copy-start(bf16[1,768,2048]{2,1,0:T(8,128)(2,1)} %param.16) | copy-start | bytes 9437188
  56.6 6.2 %copy-start.1 = (bf16[1,2048,256]{2,1,0:T(8,128)(2,1)S(1)}, bf16[1,2048,256]{2,1,0:T(8,128)(2,1)}, u32[]{:S(2)}) copy-start(bf16[1,2048,256]{2,1,0:T(8,128)(2,1)} %param.17) | copy-start | bytes 3145732
  62.8 1.2 copy-start.2
  62.8 1.3 copy-start.7
  66.7 30.0 %copy-start.8 = (bf16[256,512]{1,0:T(8,128)(2,1)S(1)}, bf16[256,512]{1,0:T(8,128)(2,1)}, u32[]{:S(2)}) copy-start(bf16[256,512]{1,0:T(8,128)(2,1)} %param.13) | copy-start | bytes 786436
  66.7 43.6 %copy-start.9 = (bf16[256,512]{1,0:T(8,128)(2,1)S(1)}, bf16[256,512]{1,0:T(8,128)(2,1)}, u32[]{:S(2)}) copy-start(bf16[256,512]{1,0:T(8,128)(2,1)} %param.21) | copy-start | bytes 786436
  66.7 43.6 %copy-start.12 = (f32[256]{0:T(256)S(1)}, f32[256]{0:T(256)}, u32[]{:S(2)}) copy-start(f32[256]{0:T(256)} %add_rsqrt_fusion.1) | copy-start | bytes 3076
  66.7 43.6 %copy-start.17 = (f32[512]{0:T(512)S(1)}, f32[512]{0:T(512)}, u32[]{:S(2)}) copy-start(f32[512]{0:T(512)} %param.22) | copy-start | bytes 6148
  110.4 3.7 %copy-start.4 = (bf16[256,2048]{1,0:T(8,128)(2,1)S(1)}, bf16[256,2048]{1,0:T(8,128)(2,1)}, u32[]{:S(2)}) copy-start(bf16[256,2048]{1,0:T(8,128)(2,1)} %shard_map.174) | copy-start | bytes 3145732
  116.4 41.8 %copy-start.10 = (bf16[256,512]{1,0:T(8,128)(2,1)S(1)}, bf16[256,512]{1,0:T(8,128)(2,1)}, u32[]{:S(2)}) copy-start(bf16[256,512]{1,0:T(8,128)(2,1)} %param.24) | copy-start | bytes 786436
  116.4 41.8 %copy-start.11 = (bf16[256,512]{1,0:T(8,128)(2,1)S(1)}, bf16[256,512]{1,0:T(8,128)(2,1)}, u32[]{:S(2)}) copy-start(bf16[256,512]{1,0:T(8,128)(2,1)} %param.25) | copy-start | bytes 786436
  155.0 3.3 %copy-start.5 = (f32[256,512]{1,0:T(8,128)S(1)}, f32[256,512]{1,0:T(8,128)}, u32[]{:S(2)}) copy-start(f32[256,512]{1,0:T(8,128)} %get-tuple-element.19) | copy-start | bytes 1572868
